TPU v7x, 32 devices: a whole 2x2x4 slice. The times are simulated.
32 devices in a mesh: grp: 2 (over x), ep: 16 (over z, y, core).
Axes of the slice: x: 2, y: 2, z: 4, core: 2. Of those that a mesh axis runs over, the one named last changes fastest.
Arguments:
- tokens: bfloat16 [512, 2048], P(('grp', 'ep')), parts along dimension 0, may hold values from -6 to 6
- attn_gain: float32 [2048], replicated, may hold values from 0.1 to 1.9
- w_query: bfloat16 [2048, 1024], replicated, may hold values from -0.125 to 0.125
- w_key: bfloat16 [2048, 128], replicated, may hold values from -0.125 to 0.125
- w_value: bfloat16 [2048, 128], replicated, may hold values from -0.125 to 0.125
- w_forget: bfloat16 [2048, 2], replicated, may hold values from -0.125 to 0.125
- forget_bias: float32 [2], replicated, may hold values from -3 to 1
- w_attn_out: bfloat16 [1024, 2048], replicated, may hold values from -0.1875 to 0.1875
- cache_keys: bfloat16 [512, 1024, 128], P(('grp', 'ep')), parts along dimension 0, may hold values from -640 to 640
- cache_values: bfloat16 [512, 1024, 128], P(('grp', 'ep')), parts along dimension 0, may hold values from -6 to 6
- cache_logsum: float32 [512, 2, 1024], P(('grp', 'ep')), parts along dimension 0, may hold values from -100 to 0, as said below
- lengths: int32 [512], P(('grp', 'ep')), parts along dimension 0, may hold values from 1 to 1024, as said below
- ffn_gain: float32 [2048], replicated, may hold values from 0.1 to 1.9
- branch_gate: float32 [2048], replicated, may hold values from -0.125 to 0.125
- dense_gate: bfloat16 [2048, 4096], P(None, 'ep'), may hold values from -0.125 to 0.125
- dense_up: bfloat16 [2048, 4096], P(None, 'ep'), may hold values from -0.125 to 0.125
- dense_down: bfloat16 [4096, 2048], P('ep'), may hold values from -0.09375 to 0.09375
- expert_gate: bfloat16 [16, 2048, 512], P('ep'), may hold values from -0.125 to 0.125
- expert_up: bfloat16 [16, 2048, 512], P('ep'), may hold values from -0.125 to 0.125
- expert_down: bfloat16 [16, 512, 2048], P('ep'), may hold values from -0.25 to 0.25
- routes: int32 [512, 4], P(('grp', 'ep')), parts along dimension 0, may hold values from 0 to 15, all different within a row; in each aligned block of 16 rows (0 to 15, 16 to 31, ...) at most 8 rows name the same one
- route_weights: float32 [512, 4], P(('grp', 'ep')), parts along dimension 0, may hold values from 0.2 to 1
Outputs:
- output_rows: bfloat16 [512, 2048], P(('grp', 'ep')), parts along dimension 0
There are 2 independent parts, one for each index of `grp`. A program takes and returns all parts, laid end to end along the dimension named above; an argument that names none is the same for every part. Nothing has to cross between parts.
Inputs may be any that keep to these rules, and one draw needn't show every extreme that they name: `lengths`: each aligned block of 16 sequences holds one with 1024 valid positions; every length is at least 128. `routes`: a row's 4 experts differ; among the rows of one device no expert is named more than 8 times. `cache_logsum`: non-increasing along positions.
All inputs are finite; a program needn't handle non-finite values.
Results may differ from a plain program's by a relative error of at most 0.012.
The roundings to bfloat16 on the way count: a program that leaves them out, or rounds other values in their place, can miss the bound.
Values may be sent and summed in bfloat16 or wider, within the bound.
No kernel may reach another device: no remote copies, remote signals or barrier semaphores. Data moves between devices by JAX's collectives and lax.ppermute only.
A program may use at most 128 MiB of HBM per device.

v0:
```python
import math

import jax
import jax.numpy as jnp
from jax import lax
from jax.sharding import PartitionSpec as P

EPSILON = 1e-06


def norm_rows(inputs, gain_vec):
    widened = inputs.astype(jnp.float32)
    scaled = widened * lax.rsqrt(jnp.mean(widened * widened, axis=-1, keepdims=True) + EPSILON)
    return (scaled * gain_vec).astype(jnp.bfloat16)


def swiglu(row_block, w_first, w_second):
    gate_part = jnp.dot(row_block, w_first, preferred_element_type=jnp.float32)
    up_part = jnp.dot(row_block, w_second, preferred_element_type=jnp.float32)
    return (jax.nn.silu(gate_part) * up_part).astype(jnp.bfloat16)


def expert_rows(row_block, w_gate, w_up, w_down):
    middle = swiglu(row_block, w_gate, w_up)
    return jnp.dot(middle, w_down, preferred_element_type=jnp.float32).astype(jnp.bfloat16)


def attend(
    normed,
    w_query,
    w_key,
    w_value,
    w_forget,
    forget_bias,
    cache_keys,
    cache_values,
    cache_logsum,
    lengths,
):
    own_rows = normed.shape[0]
    kv_heads = cache_logsum.shape[1]
    cache_span = cache_logsum.shape[2]
    head_size = w_key.shape[1] // kv_heads
    group_size = w_query.shape[1] // head_size // kv_heads
    scaling = 1.0 / math.sqrt(head_size)
    queries = jnp.dot(normed, w_query, preferred_element_type=jnp.float32).astype(jnp.bfloat16)
    new_keys = jnp.dot(normed, w_key, preferred_element_type=jnp.float32).astype(jnp.bfloat16)
    new_values = jnp.dot(normed, w_value, preferred_element_type=jnp.float32).astype(jnp.bfloat16)
    log_gate = jax.nn.log_sigmoid(
        jnp.dot(normed, w_forget, preferred_element_type=jnp.float32) + forget_bias
    )
    positions = lax.broadcasted_iota(jnp.int32, (own_rows, kv_heads, cache_span), 2)
    latest = jnp.sum(jnp.where(positions == lengths[:, None, None] - 1, cache_logsum, 0.0), axis=2)
    offsets = (latest + log_gate)[:, :, None] - cache_logsum
    usable = positions < lengths[:, None, None]
    query_heads = queries.reshape(own_rows, kv_heads, group_size, head_size)
    key_heads = cache_keys.reshape(own_rows, cache_span, kv_heads, head_size)
    value_heads = cache_values.reshape(own_rows, cache_span, kv_heads, head_size)
    scores = (
        jnp.einsum("bgrd,blgd->bgrl", query_heads, key_heads, preferred_element_type=jnp.float32)
        * scaling
    )
    scores = jnp.where(usable[:, :, None, :], scores + offsets[:, :, None, :], -jnp.inf)
    self_score = (
        jnp.einsum(
            "bgrd,bgd->bgr",
            query_heads,
            new_keys.reshape(own_rows, kv_heads, head_size),
            preferred_element_type=jnp.float32,
        )
        * scaling
    )
    peak_score = jnp.maximum(jnp.max(scores, axis=3), self_score)
    cache_weight = jnp.exp(scores - peak_score[..., None])
    self_weight = jnp.exp(self_score - peak_score)
    denominator = jnp.sum(cache_weight, axis=3) + self_weight
    cache_probs = (cache_weight / denominator[..., None]).astype(jnp.bfloat16)
    self_probs = (self_weight / denominator).astype(jnp.bfloat16)
    attended = jnp.einsum(
        "bgrl,blgd->bgrd", cache_probs, value_heads, preferred_element_type=jnp.float32
    )
    attended = attended + self_probs.astype(jnp.float32)[..., None] * new_values.reshape(
        own_rows, kv_heads, 1, head_size
    ).astype(jnp.float32)
    return attended.reshape(own_rows, -1).astype(jnp.bfloat16)


def body(
    tokens,
    attn_gain,
    w_query,
    w_key,
    w_value,
    w_forget,
    forget_bias,
    w_attn_out,
    cache_keys,
    cache_values,
    cache_logsum,
    lengths,
    ffn_gain,
    branch_gate,
    dense_gate,
    dense_up,
    dense_down,
    expert_gate,
    expert_up,
    expert_down,
    routes,
    route_weights,
):
    own_rows = tokens.shape[0]
    normed = norm_rows(tokens, attn_gain)
    attended = attend(
        normed,
        w_query,
        w_key,
        w_value,
        w_forget,
        forget_bias,
        cache_keys,
        cache_values,
        cache_logsum,
        lengths,
    )
    residual = tokens.astype(jnp.float32) + jnp.dot(
        attended, w_attn_out, preferred_element_type=jnp.float32
    )
    second = norm_rows(residual, ffn_gain)
    branch_share = jax.nn.sigmoid(
        jnp.dot(second.astype(jnp.float32), branch_gate, precision=lax.Precision.HIGHEST)
    )
    expert_count = lax.axis_size("ep")
    route_count = routes.shape[1]
    capacity = max(2, 2 * own_rows * route_count // expert_count)
    hits = (
        routes[:, :, None]
        == lax.broadcasted_iota(jnp.int32, (own_rows, route_count, expert_count), 2)
    ).astype(jnp.int32)
    flat_hits = hits.reshape(own_rows * route_count, expert_count)
    order_rank = jnp.sum((jnp.cumsum(flat_hits, axis=0) - 1) * flat_hits, axis=1).reshape(
        own_rows, route_count
    )
    slot_index = routes * capacity + order_rank
    slot_total = expert_count * capacity
    matches = slot_index[None, :, :] == lax.broadcasted_iota(
        jnp.int32, (slot_total, own_rows, route_count), 0
    )
    dispatch = jnp.sum(matches.astype(jnp.float32), axis=2).astype(jnp.bfloat16)
    combine = jnp.sum(jnp.where(matches, route_weights[None, :, :], 0.0), axis=2).T
    outgoing = jnp.dot(dispatch, second, preferred_element_type=jnp.float32).astype(jnp.bfloat16)
    outgoing = outgoing.reshape(expert_count, 1, capacity, -1)
    arrived = lax.all_to_all(outgoing, "ep", split_axis=0, concat_axis=1, tiled=True)
    arrived_shape = arrived.shape
    answer = expert_rows(
        arrived.reshape(-1, arrived_shape[3]), expert_gate[0], expert_up[0], expert_down[0]
    )
    returned = lax.all_to_all(
        answer.reshape(arrived_shape), "ep", split_axis=1, concat_axis=0, tiled=True
    )
    routed = jnp.dot(
        combine,
        returned.reshape(slot_total, -1).astype(jnp.float32),
        precision=lax.Precision.HIGHEST,
    )
    dense_hidden = swiglu(lax.all_gather(second, "ep", axis=0, tiled=True), dense_gate, dense_up)
    dense = lax.psum_scatter(
        jnp.dot(dense_hidden, dense_down, preferred_element_type=jnp.float32).astype(jnp.bfloat16),
        "ep",
        scatter_dimension=0,
        tiled=True,
    ).astype(jnp.float32)
    output_rows = residual + branch_share[:, None] * dense + routed
    return output_rows.astype(jnp.bfloat16)


def solution(mesh):
    return jax.shard_map(
        body,
        mesh=mesh,
        in_specs=(
            P(("grp", "ep"), None),
            P(),
            P(),
            P(),
            P(),
            P(),
            P(),
            P(),
            P(("grp", "ep"), None, None),
            P(("grp", "ep"), None, None),
            P(("grp", "ep"), None, None),
            P(("grp", "ep")),
            P(),
            P(),
            P(None, "ep"),
            P(None, "ep"),
            P("ep", None),
            P("ep", None, None),
            P("ep", None, None),
            P("ep", None, None),
            P(("grp", "ep"), None),
            P(("grp", "ep"), None),
        ),
        out_specs=P(("grp", "ep"), None),
        check_vma=False,
    )
```

profile of v0, /device:TPU:0, one launch (start us, length us, event | category | flops | bytes accessed | tf_op | source)
XLA Modules:
  0.0 152.9 jit_solution(14952245672474803569)
XLA Ops:
  6.5 0.0 copy-start
  6.5 0.0 copy-start.11
  6.6 0.0 all-gather.2.cloned.1.call-start
  6.6 0.8 broadcast_add_fusion
  7.4 0.8 iota_compare_fusion
  8.2 1.0 fusion.43
  9.2 2.9 %convolution_convert_fusion.3 = bf16[16,1024]{1,0:T(8,128)(2,1)S(1)} fusion(bf16[2048,1024]{1,0:T(8,128)(2,1)} %param.24, bf16[16,2048]{1,0:T(8,128)(2,1)} %param.22, f32[2048]{0:T(1024)} %param.23, f32[16]{0:T(128)S(1)} %add_rsqrt_fusion.1), kind=kOutput, calls=%fused_computation.22 | convolution fusion | flops 67256320 | bytes 4300864 | tf_op jit(solution)/shard_map/dot_general | solution.py:46
  12.1 0.1 reshape.95
  12.3 0.0 copy-done.4
  12.3 0.2 fusion.46
  12.5 0.1 copy.54
  12.6 0.0 copy-done.1
  12.6 0.0 copy-done.5
  12.6 0.0 copy-done.9
  12.6 0.0 copy-done.11
  12.6 0.2 fusion.53
  12.8 0.1 copy.55
  12.9 0.1 broadcast_subtract_fusion
  13.0 0.0 copy-start.3
  13.0 6.5 %copy.53 = bf16[16,1024,128]{1,2,0:T(8,128)(2,1)} copy(bf16[16,1024,128]{2,1,0:T(8,128)(2,1)} %param.30) | data formatting | bytes 8388608 | tf_op args[8]
  19.5 0.0 copy-done.3
  19.5 0.2 convolution_convert_fusion.5
  19.7 0.1 reshape.109
  19.8 0.2 fusion.62
  20.0 3.0 %fusion.61 = (f32[16,2,8]{2,1,0:T(2,128)S(1)}, f32[16,2,8,1024]{3,2,1,0:T(8,128)S(1)}) fusion(f32[16,2,1024]{2,1,0:T(2,128)S(1)} %broadcast_subtract_fusion, bf16[16,2,8,64]{3,2,1,0:T(8,128)(2,1)S(1)} %reshape.95, bf16[16,1024,2,64]{1,3,2,0:T(8,128)(2,1)} %bitcast.70, pred[16,2,1024]{2,1,0:T(4,128)(4,1)S(1)} %iota_compare_fusion), kind=kOutput, calls=%fused_computation.85 | convolution fusion | flops 34602752 | bytes 5440512 | tf_op jit(solution)/shard_map/bgrd,blgd->bgrl/dot_general | solution.py:60
  23.0 0.3 fusion.24
  23.3 1.3 fusion.18
  24.6 0.1 reshape.103
  24.7 6.4 %copy.56 = bf16[16,1024,128]{1,2,0:T(8,128)(2,1)} copy(bf16[16,1024,128]{2,1,0:T(8,128)(2,1)} %param.31) | data formatting | bytes 8388608 | tf_op args[9]
  31.1 3.4 %fusion.17 = bf16[16,2,8,64]{3,2,1,0:T(8,128)(2,1)S(1)} fusion(bf16[16,1024,2,64]{1,3,2,0:T(8,128)(2,1)} %bitcast.71, f32[16,2,8,1024]{3,2,1,0:T(8,128)S(1)} %get-tuple-element.10, f32[16,2,8]{2,1,0:T(2,128)S(1)} %get-tuple-element.8, f32[16,2,8]{2,1,0:T(2,128)S(1)} %multiply_maximum_fusion, f32[16,2,64]{2,1,0:T(2,128)S(1)} %reshape.103, ...), kind=kOutput, calls=%fused_computation.21 | convolution fusion | flops 34390016 | bytes 5286912 | tf_op jit(solution)/shard_map/bgrl,blgd->bgrd/dot_general | solution.py:79
  34.5 0.1 convert_element_type.90
  34.7 3.0 %multiply_reduce_fusion = (f32[16]{0:T(128)S(1)}, f32[16,2048]{1,0:T(8,128)S(1)}) fusion(bf16[16,1024]{1,0:T(8,128)(2,1)S(1)} %convert_element_type.90, bf16[1024,2048]{1,0:T(8,128)(2,1)} %param.29, bf16[16,2048]{1,0:T(8,128)(2,1)S(1)} %copy-done.1), kind=kOutput, calls=%fused_computation.61 | convolution fusion | flops 67239920 | bytes 4423744 | tf_op jit(solution)/shard_map/dot_general | solution.py:126
  37.6 0.0 copy-done.6
  37.7 0.7 multiply_convert_fusion
  38.4 0.0 all-gather.2.cloned.1.call-update
  38.4 0.0 copy-done.7
  38.4 0.1 copy.57
  38.5 0.1 eq.31
  38.6 0.1 fusion.49
  38.7 0.1 reduce_window_sum.11
  38.8 0.2 select_reduce_fusion.1
  38.9 0.1 reduce_sum.70
  39.0 0.1 copy.58
  39.1 0.0 copy-done.8
  39.1 0.1 convert_reduce_fusion
  39.2 2.0 %fusion = bf16[16,1,8,2048]{3,2,1,0:T(8,128)(2,1)} fusion(bf16[16,2048]{1,0:T(8,128)(2,1)} %multiply_convert_fusion, bf16[128,16]{0,1:T(8,128)(2,1)S(1)} %get-tuple-element.5), kind=kOutput, calls=%fused_computation.3 | convolution fusion | flops 8650752 | bytes 593920 | tf_op jit(solution)/shard_map/dot_general | solution.py:151
  41.2 7.4 %all-to-all-start = ((bf16[16,1,8,2048]{3,2,1,0:T(8,128)(2,1)}), bf16[16,1,8,2048]{3,2,1,0:T(8,128)(2,1)S(1)}, u32[]{:S(2)}, u32[]{:S(2)}) async-start(bf16[16,1,8,2048]{3,2,1,0:T(8,128)(2,1)} %fusion), calls=%async_computation.1 | async-start | bytes 1048576 | tf_op jit(solution)/shard_map/all_to_all | solution.py:153
  48.6 0.0 reduce-scatter.2.cloned.1.call-start
  48.6 32.8 %all-gather.2.cloned.1.call-done = bf16[256,2048]{1,0:T(8,128)(2,1)} async-done(((bf16[16,2048]{1,0:T(8,128)(2,1)}), bf16[256,2048]{1,0:T(8,128)(2,1)}) %all-gather.2.cloned.1.call-update) | async-done | bytes 1048592 | tf_op jit(solution)/shard_map/all_gather | solution.py:166
  81.5 2.0 %fusion.63 = f32[256,256]{1,0:T(8,128)S(1)} fusion(bf16[256,2048]{1,0:T(8,128)(2,1)} %all-gather.2.cloned.1.call-done, bf16[2048,256]{1,0:T(8,128)(2,1)} %param.36), kind=kOutput, calls=%fused_computation.87 | convolution fusion | flops 268435456 | bytes 2359296 | tf_op jit(solution)/shard_map/dot_general | solution.py:18
  83.4 4.1 %convolution_convert_fusion = bf16[256,2048]{1,0:T(8,128)(2,1)} fusion(bf16[256,2048]{1,0:T(8,128)(2,1)} %param.38, bf16[256,2048]{1,0:T(8,128)(2,1)} %all-gather.2.cloned.1.call-done, bf16[2048,256]{1,0:T(8,128)(2,1)} %param.37, f32[256,256]{1,0:T(8,128)S(1)} %fusion.63), kind=kOutput, calls=%fused_computation | convolution fusion | flops 537788416 | bytes 4456448 | tf_op jit(solution)/shard_map/dot_general | solution.py:168
  87.6 0.0 reduce-scatter.2.cloned.1.call-update
  87.6 0.0 copy-start.2
  87.6 0.0 copy-start.10
  87.6 0.0 all-to-all-done
  87.6 2.0 %fusion.6 = f32[128,512]{1,0:T(8,128)S(1)} fusion(bf16[1,2048,512]{2,1,0:T(8,128)(2,1)} %param.39, bf16[16,1,8,2048]{3,2,1,0:T(8,128)(2,1)S(1)} %all-to-all-done), kind=kOutput, calls=%fused_computation.11 | convolution fusion | flops 268435456 | bytes 2883584 | tf_op jit(solution)/shard_map/dot_general | solution.py:18
  89.7 0.0 copy-done
  89.7 3.2 %fusion.1 = bf16[1,16,8,2048]{3,2,0,1:T(8,128)(2,1)} fusion(bf16[1,512,2048]{2,1,0:T(8,128)(2,1)S(1)} %copy-done, bf16[1,2048,512]{2,1,0:T(8,128)(2,1)} %param.40, bf16[16,1,8,2048]{3,2,1,0:T(8,128)(2,1)S(1)} %all-to-all-done, f32[128,512]{1,0:T(8,128)S(1)} %fusion.6), kind=kOutput, calls=%fused_computation.4 | convolution fusion | flops 537526272 | bytes 5505024 | tf_op jit(solution)/shard_map/dot_general | solution.py:25
  92.9 3.7 %all-to-all-start.1 = ((bf16[1,16,8,2048]{3,2,0,1:T(8,128)(2,1)}), bf16[1,16,8,2048]{3,2,0,1:T(8,128)(2,1)S(1)}, u32[]{:S(2)}, u32[]{:S(2)}) async-start(bf16[1,16,8,2048]{3,2,0,1:T(8,128)(2,1)} %fusion.1), calls=%async_computation.2 | async-start | bytes 1048576 | tf_op jit(solution)/shard_map/all_to_all | solution.py:158
  96.6 0.0 copy-done.2
  96.7 0.1 fusion.23
  96.8 14.1 %all-to-all-done.1 = bf16[1,16,8,2048]{3,2,0,1:T(8,128)(2,1)S(1)} async-done(((bf16[1,16,8,2048]{3,2,0,1:T(8,128)(2,1)}), bf16[1,16,8,2048]{3,2,0,1:T(8,128)(2,1)S(1)}, u32[]{:S(2)}, u32[]{:S(2)}) %all-to-all-start.1) | async-done | bytes 524320 | tf_op jit(solution)/shard_map/all_to_all | solution.py:158
  110.9 33.4 %reduce-scatter.2.cloned.1.call-done = bf16[16,2048]{1,0:T(8,128)(2,1)} async-done(((bf16[256,2048]{1,0:T(8,128)(2,1)}), bf16[16,2048]{1,0:T(8,128)(2,1)}) %reduce-scatter.2.cloned.1.call-update) | async-done | bytes 65552 | tf_op jit(solution)/shard_map/reduce_scatter | solution.py:167
  144.3 1.8 %fusion.2 = bf16[16,2048]{1,0:T(8,128)(2,1)} fusion(f32[128,16]{0,1:T(8,128)S(1)} %get-tuple-element.6, bf16[1,16,8,2048]{3,2,0,1:T(8,128)(2,1)S(1)} %all-to-all-done.1, f32[16,2048]{1,0:T(8,128)S(1)} %get-tuple-element.12, bf16[16,2048]{1,0:T(8,128)(2,1)} %reduce-scatter.2.cloned.1.call-done, f32[16]{0:T(128)S(1)} %fusion.23), kind=kOutput, calls=%fused_computation.7 | convolution fusion | flops 50495488 | bytes 794688 | tf_op jit(solution)/shard_map/dot_general | solution.py:161
  (13 shorter events, 0.1 us)
Async XLA Ops:
  6.5 83.2 %copy-start = (bf16[1,512,2048]{2,1,0:T(8,128)(2,1)S(1)}, bf16[1,512,2048]{2,1,0:T(8,128)(2,1)}, u32[]{:S(2)}) copy-start(bf16[1,512,2048]{2,1,0:T(8,128)(2,1)} %param.41) | copy-start | bytes 6291460
  6.5 6.0 %copy-start.1 = (bf16[16,2048]{1,0:T(8,128)(2,1)S(1)}, bf16[16,2048]{1,0:T(8,128)(2,1)}, u32[]{:S(2)}) copy-start(bf16[16,2048]{1,0:T(8,128)(2,1)} %param.22) | copy-start | bytes 196612
  6.5 6.0 %copy-start.5 = (f32[2048]{0:T(1024)S(1)}, f32[2048]{0:T(1024)}, u32[]{:S(2)}) copy-start(f32[2048]{0:T(1024)} %param.23) | copy-start | bytes 24580
  6.5 5.7 %copy-start.4 = (f32[16,2,1024]{2,1,0:T(2,128)S(1)}, f32[16,2,1024]{2,1,0:T(2,128)}, u32[]{:S(2)}) copy-start(f32[16,2,1024]{2,1,0:T(2,128)} %param.32) | copy-start | bytes 393220
  6.5 6.0 %copy-start.9 = (bf16[2048,2]{0,1:T(2,128)(2,1)S(1)}, bf16[2048,2]{0,1:T(2,128)(2,1)}, u32[]{:S(2)}) copy-start(bf16[2048,2]{0,1:T(2,128)(2,1)} %param.27) | copy-start | bytes 24580
  6.5 6.0 %copy-start.11 = (f32[2]{0:T(128)S(1)}, f32[2]{0:T(128)}, u32[]{:S(2)}) copy-start(f32[2]{0:T(128)} %param.28) | copy-start | bytes 28
  6.6 74.9 %all-gather.2.cloned.1.call-start = ((), (), s32[]{:S(2)}) async-start(), calls=%async_computation.3 | async-start | bytes 1114112 | tf_op jit(solution)/shard_map/all_gather | solution.py:166
  13.0 6.5 %copy-start.3 = (bf16[2048,128]{1,0:T(8,128)(2,1)S(1)}, bf16[2048,128]{1,0:T(8,128)(2,1)}, u32[]{:S(2)}) copy-start(bf16[2048,128]{1,0:T(8,128)(2,1)} %param.25) | copy-start | bytes 1572868
  31.1 6.6 %copy-start.6 = (f32[2048]{0:T(1024)S(1)}, f32[2048]{0:T(1024)}, u32[]{:S(2)}) copy-start(f32[2048]{0:T(1024)} %param.34) | copy-start | bytes 24580
  34.5 3.9 %copy-start.7 = (s32[16,4]{0,1:T(4,128)S(1)}, s32[16,4]{0,1:T(4,128)}, u32[]{:S(2)}) copy-start(s32[16,4]{0,1:T(4,128)} %param.42) | copy-start | bytes 772
  34.5 4.6 %copy-start.8 = (f32[16,4]{0,1:T(4,128)S(1)}, f32[16,4]{0,1:T(4,128)}, u32[]{:S(2)}) copy-start(f32[16,4]{0,1:T(4,128)} %param.43) | copy-start | bytes 772
  41.2 46.4 %all-to-all-start = ((bf16[16,1,8,2048]{3,2,1,0:T(8,128)(2,1)}), bf16[16,1,8,2048]{3,2,1,0:T(8,128)(2,1)S(1)}, u32[]{:S(2)}, u32[]{:S(2)}) async-start(bf16[16,1,8,2048]{3,2,1,0:T(8,128)(2,1)} %fusion), calls=%async_computation.1 | async-start | bytes 1048576 | tf_op jit(solution)/shard_map/all_to_all | solution.py:153
  48.6 95.7 %reduce-scatter.2.cloned.1.call-start = ((), (), s32[]{:S(2)}) async-start(), calls=%async_computation.4 | async-start | bytes 1114112 | tf_op jit(solution)/shard_map/reduce_scatter | solution.py:167
  87.6 9.0 %copy-start.2 = (bf16[16,2048]{1,0:T(8,128)(2,1)S(1)}, bf16[16,2048]{1,0:T(8,128)(2,1)}, u32[]{:S(2)}) copy-start(bf16[16,2048]{1,0:T(8,128)(2,1)} %multiply_convert_fusion) | copy-start | bytes 196612
  87.6 9.0 %copy-start.10 = (f32[2048]{0:T(1024)S(1)}, f32[2048]{0:T(1024)}, u32[]{:S(2)}) copy-start(f32[2048]{0:T(1024)} %param.35) | copy-start | bytes 24580
  92.9 18.0 %all-to-all-start.1 = ((bf16[1,16,8,2048]{3,2,0,1:T(8,128)(2,1)}), bf16[1,16,8,2048]{3,2,0,1:T(8,128)(2,1)S(1)}, u32[]{:S(2)}, u32[]{:S(2)}) async-start(bf16[1,16,8,2048]{3,2,0,1:T(8,128)(2,1)} %fusion.1), calls=%async_computation.2 | async-start | bytes 1048576 | tf_op jit(solution)/shard_map/all_to_all | solution.py:158
Sparse Core Ops, SparseCore 0:
  38.5 42.8 all-gather.1
  87.7 56.5 reduce-scatter.1
where the time goes:
time: 154 us; the launch traced here: 153 us
  waiting for transfers between devices  80.4 us (52%)
  matrix products  29.5 us (19%)
  local copies, waits for them, and re-layouts  13.8 us (9%)
  between operations  13.6 us (9%)
  starting transfers between devices  11.2 us (7%)
  other arithmetic  4.46 us (3%)
    reduce_scatter x1, waiting for transfers between devices, body(): lax.psum_scatter(jnp.dot(dense_hidden, dense_down, preferred_element_type...  33.4 us
    all_gather x1, waiting for transfers between devices, body(): lax.all_gather(second, 'ep', axis=0, tiled=True)  32.8 us
    all_to_all x1, waiting for transfers between devices, body(): lax.all_to_all(answer.reshape(arrived_shape), 'ep', split_axis=1, concat_...  14.1 us
    unnamed x27, local copies, waits for them, and re-layouts  13 us
    all_to_all x1, starting transfers between devices, body(): lax.all_to_all(outgoing, 'ep', split_axis=0, concat_axis=1, tiled=True)  7.41 us
    dot_general x1, matrix products, body(): jnp.dot(dense_hidden, dense_down, preferred_element_type=jnp.float32)  4.14 us
    dot_general x2, matrix products, swiglu(): gate_part = jnp.dot(row_block, w_first, preferred_element_type=jnp.float32)  4.02 us
    all_to_all x1, starting transfers between devices, body(): lax.all_to_all(answer.reshape(arrived_shape), 'ep', split_axis=1, concat_...  3.68 us
  transfers between devices with their start and end apart: 4, of which 3 were waited for; matrix products, arithmetic and copies ran while one was open for 9% of the time, Pallas kernels for 0%

commit v1 on v0

v1 whole, which is shorter than its diff:
```python
import math

import jax
import jax.numpy as jnp
from jax import lax
from jax.experimental import pallas as pl
from jax.experimental.pallas import tpu as pltpu
from jax.sharding import PartitionSpec as P

EPSILON = 1e-06
META = 128
NT = (((1,), (1,)), ((), ()))


def mm(a, b):
    return jnp.dot(a, b, preferred_element_type=jnp.float32)


def norm_block(widened, gain):
    scaled = widened * lax.rsqrt(jnp.mean(widened * widened, axis=-1, keepdims=True) + EPSILON)
    return (scaled * gain).astype(jnp.bfloat16)


def attention_kernel(
    lengths_ref, bias_ref, tokens_ref, attn_gain_ref, forget_ref, ffn_gain_ref, meta_ref,
    wq_hbm, wk_hbm, wv_hbm, wo_hbm, keys_hbm, values_hbm, logsum_hbm,
    residual_ref, second_ref,
    wq, wk, wv, wo, keys, values, logsum, masked_q, attended, weight_sems, cache_sems,
):
    rows, width = tokens_ref.shape
    kv_heads, span = logsum.shape[1], logsum.shape[2]
    kv_width = wk.shape[1]
    head_size = kv_width // kv_heads
    heads = wq.shape[1] // head_size
    group = heads // kv_heads
    shift = head_size.bit_length() - 1
    scaling = 1.0 / math.sqrt(head_size)
    loads = [
        pltpu.make_async_copy(s, d, weight_sems.at[i])
        for i, (s, d) in enumerate(
            ((wq_hbm, wq), (wk_hbm, wk), (wv_hbm, wv), (logsum_hbm, logsum), (wo_hbm, wo))
        )
    ]
    key_loads = [
        pltpu.make_async_copy(keys_hbm.at[b], keys.at[b], cache_sems.at[0, b]) for b in range(rows)
    ]
    value_loads = [
        pltpu.make_async_copy(values_hbm.at[b], values.at[b], cache_sems.at[1, b])
        for b in range(rows)
    ]
    for load in loads[:4]:
        load.start()
    for b in range(rows):
        key_loads[b].start()
        value_loads[b].start()
    loads[4].start()

    tokens = tokens_ref[...].astype(jnp.float32)
    normed = norm_block(tokens, attn_gain_ref[...])
    normed_wide = normed.astype(jnp.float32)
    log_gates = []
    for g in range(kv_heads):
        logit = (
            jnp.sum(normed_wide * forget_ref[g : g + 1, :].astype(jnp.float32), axis=1, keepdims=True)
            + bias_ref[g]
        )
        log_gates.append(jnp.minimum(logit, 0.0) - jnp.log1p(jnp.exp(-jnp.abs(logit))))

    lane = lax.broadcasted_iota(jnp.int32, (heads, wq.shape[1]), 1)
    own_head = lax.broadcasted_iota(jnp.int32, (heads, wq.shape[1]), 0) == (lane >> shift)
    fold_row = lax.broadcasted_iota(jnp.int32, (wq.shape[1], kv_width), 0)
    fold_lane = lax.broadcasted_iota(jnp.int32, (wq.shape[1], kv_width), 1)
    fold_target = (fold_row & (head_size - 1)) + (
        (fold_row >> (shift + group.bit_length() - 1)) << shift
    )
    fold = (fold_lane == fold_target).astype(jnp.float32).astype(jnp.bfloat16)

    loads[0].wait()
    queries = mm(normed, wq[...]).astype(jnp.bfloat16).astype(jnp.float32) * scaling
    for b in range(rows):
        masked_q[b * heads : (b + 1) * heads, :] = jnp.where(
            own_head, queries[b : b + 1, :], 0.0
        ).astype(jnp.bfloat16)
    spread_q = mm(masked_q[...], fold)
    spread_q16 = spread_q.astype(jnp.bfloat16)
    loads[1].wait()
    new_keys = mm(normed, wk[...]).astype(jnp.bfloat16).astype(jnp.float32)
    loads[2].wait()
    new_values = mm(normed, wv[...]).astype(jnp.bfloat16).astype(jnp.float32)
    loads[3].wait()
    position = lax.broadcasted_iota(jnp.int32, (1, span), 1)

    step = math.gcd(rows, 4)
    for first in range(0, rows, step):
        members = range(first, first + step)
        for b in members:
            key_loads[b].wait()
        raw = [
            lax.dot_general(
                spread_q16[b * heads : (b + 1) * heads, :], keys[b], NT,
                preferred_element_type=jnp.float32,
            )
            for b in members
        ]
        probs = []
        for b, score in zip(members, raw):
            length = lengths_ref[b]
            parts = []
            for g in range(kv_heads):
                decay = logsum[b, g : g + 1, :]
                latest = jnp.sum(jnp.where(position == length - 1, decay, 0.0), axis=1, keepdims=True)
                total = latest + log_gates[g][b : b + 1, :]
                offset = jnp.where(position < length, total - decay, -jnp.inf)
                parts.append(score[g * group : (g + 1) * group, :] + offset)
            score = jnp.concatenate(parts, axis=0)
            own = jnp.sum(
                spread_q[b * heads : (b + 1) * heads, :] * new_keys[b : b + 1, :],
                axis=1, keepdims=True,
            )
            peak = jnp.maximum(jnp.max(score, axis=1, keepdims=True), own)
            weight = jnp.exp(score - peak)
            own_weight = jnp.exp(own - peak)
            inverse = 1.0 / (jnp.sum(weight, axis=1, keepdims=True) + own_weight)
            probs.append(
                (
                    (weight * inverse).astype(jnp.bfloat16),
                    (own_weight * inverse).astype(jnp.bfloat16).astype(jnp.float32),
                )
            )
        for b in members:
            value_loads[b].wait()
        for b, (prob, own_prob) in zip(members, probs):
            mixed = mm(prob, values[b]) + own_prob * new_values[b : b + 1, :]
            attended[b * heads : (b + 1) * heads, :] = mixed.astype(jnp.bfloat16)

    wide = lax.dot_general(attended[...], fold, NT, preferred_element_type=jnp.float32)
    wide = jnp.where(own_head[None], wide.reshape(rows, heads, -1), 0.0)
    side = jnp.sum(wide, axis=1).astype(jnp.bfloat16)
    loads[4].wait()
    residual = tokens + mm(side, wo[...])
    residual_ref[...] = residual
    second_ref[:, :width] = norm_block(residual, ffn_gain_ref[...])
    second_ref[:, width:] = meta_ref[...]


def attention(
    tokens, attn_gain, w_query, w_key, w_value, w_forget, forget_bias, w_attn_out,
    cache_keys, cache_values, cache_logsum, lengths, ffn_gain, meta,
):
    rows, width = tokens.shape
    heads = w_query.shape[1] // (w_key.shape[1] // cache_logsum.shape[1])
    smem = pl.BlockSpec(memory_space=pltpu.SMEM)
    vmem = pl.BlockSpec(memory_space=pltpu.VMEM)
    hbm = pl.BlockSpec(memory_space=pl.ANY)
    return pl.pallas_call(
        attention_kernel,
        out_shape=(
            jax.ShapeDtypeStruct((rows, width), jnp.float32),
            jax.ShapeDtypeStruct((rows, width + META), jnp.bfloat16),
        ),
        in_specs=[smem, smem] + [vmem] * 5 + [hbm] * 7,
        out_specs=(vmem, vmem),
        scratch_shapes=[
            pltpu.VMEM(a.shape, a.dtype)
            for a in (w_query, w_key, w_value, w_attn_out, cache_keys, cache_values, cache_logsum)
        ]
        + [
            pltpu.VMEM((rows * heads, w_query.shape[1]), jnp.bfloat16),
            pltpu.VMEM((rows * heads, w_key.shape[1]), jnp.bfloat16),
            pltpu.SemaphoreType.DMA((5,)),
            pltpu.SemaphoreType.DMA((2, rows)),
        ],
        compiler_params=pltpu.CompilerParams(vmem_limit_bytes=36 << 20),
        name="attention",
    )(
        lengths, forget_bias, tokens, attn_gain[None], w_forget.T, ffn_gain[None], meta,
        w_query, w_key, w_value, w_attn_out, cache_keys, cache_values, cache_logsum,
    )


def feed_forward_kernel(top, piece_count, *refs):
    own_ref, gate_ref = refs[:2]
    pieces = refs[2 : 2 + piece_count]
    sources = refs[2 + piece_count : 8 + piece_count]
    outs = refs[8 + piece_count : -8]
    buffers = refs[-8:-2]
    x_ref, sems = refs[-2:]
    dense_gate, dense_up, expert_gate, expert_up, dense_down, expert_down = buffers
    loads = [
        pltpu.make_async_copy(s, d, sems.at[i]) for i, (s, d) in enumerate(zip(sources, buffers))
    ]
    for load in loads:
        load.start()
    width = dense_gate.shape[0]
    at = 0
    meta = []
    for piece in pieces:
        block = piece[...].reshape(-1, width + META)
        x_ref[at : at + block.shape[0], :] = block[:, :width]
        meta.append(block[:, width:])
        at += block.shape[0]
    meta = jnp.concatenate(meta, axis=0).astype(jnp.float32)
    weights = (
        meta[:, top : 2 * top] + meta[:, 2 * top : 3 * top] + meta[:, 3 * top : 4 * top]
    )
    own = own_ref[0].astype(jnp.float32)
    routed_weight = jnp.sum(
        jnp.where(meta[:, :top] == own, weights, 0.0), axis=1, keepdims=True
    )
    x = x_ref[...]
    share = jax.nn.sigmoid(
        jnp.sum(x.astype(jnp.float32) * gate_ref[...], axis=1, keepdims=True)
    )
    loads[0].wait()
    loads[1].wait()
    hidden = (jax.nn.silu(mm(x, dense_gate[...])) * mm(x, dense_up[...])).astype(jnp.bfloat16)
    loads[2].wait()
    loads[3].wait()
    middle = (jax.nn.silu(mm(x, expert_gate[...])) * mm(x, expert_up[...])).astype(jnp.bfloat16)
    loads[4].wait()
    loads[5].wait()
    chunk = math.gcd(width, 512)
    for c in range(0, width, chunk):
        dense = mm(hidden, dense_down[:, c : c + chunk])
        routed = mm(middle, expert_down[:, c : c + chunk]).astype(jnp.bfloat16).astype(jnp.float32)
        total = (share * dense + routed_weight * routed).astype(jnp.bfloat16)
        at = 0
        for out in outs:
            blocks, rows = out.shape[0], out.shape[1]
            out[:, :, c : c + chunk] = total[at : at + blocks * rows, :].reshape(blocks, rows, chunk)
            at += blocks * rows


def feed_forward(own, branch_gate, pieces, top, weights, out_counts):
    rows = pieces[0].shape[1]
    width = weights[0].shape[0]
    total = sum(p.shape[0] for p in pieces) * rows
    smem = pl.BlockSpec(memory_space=pltpu.SMEM)
    vmem = pl.BlockSpec(memory_space=pltpu.VMEM)
    hbm = pl.BlockSpec(memory_space=pl.ANY)

    def kernel(*refs):
        feed_forward_kernel(top, len(pieces), *refs)

    return pl.pallas_call(
        kernel,
        out_shape=tuple(
            jax.ShapeDtypeStruct((c, rows, width), jnp.bfloat16) for c in out_counts
        ),
        in_specs=[smem, vmem] + [vmem] * len(pieces) + [hbm] * 6,
        out_specs=(vmem,) * len(out_counts),
        scratch_shapes=[pltpu.VMEM(w.shape, w.dtype) for w in weights]
        + [pltpu.VMEM((total, width), jnp.bfloat16), pltpu.SemaphoreType.DMA((6,))],
        compiler_params=pltpu.CompilerParams(vmem_limit_bytes=36 << 20),
        name="feed_forward",
    )(own, branch_gate[None], *pieces, *weights)


def swap(block, mask):
    size = lax.axis_size("ep")
    return lax.ppermute(block, "ep", [(i, i ^ mask) for i in range(size)])


def wide_sum(first, *others):
    total = first.astype(jnp.float32)
    for other in others:
        total = total + other.astype(jnp.float32)
    return total


def body(
    tokens, attn_gain, w_query, w_key, w_value, w_forget, forget_bias, w_attn_out,
    cache_keys, cache_values, cache_logsum, lengths, ffn_gain, branch_gate,
    dense_gate, dense_up, dense_down, expert_gate, expert_up, expert_down,
    routes, route_weights,
):
    size = lax.axis_size("ep")
    top = routes.shape[1]
    high = lax.reduce_precision(route_weights, 8, 7)
    middle = lax.reduce_precision(route_weights - high, 8, 7)
    low = route_weights - high - middle
    meta = jnp.concatenate([routes.astype(jnp.float32), high, middle, low], axis=1)
    meta = jnp.pad(meta, ((0, 0), (0, META - 4 * top))).astype(jnp.bfloat16)
    residual, second = attention(
        tokens, attn_gain, w_query, w_key, w_value, w_forget, forget_bias, w_attn_out,
        cache_keys, cache_values, cache_logsum, lengths, ffn_gain, meta,
    )
    far = [4 * k for k in range(1, size // 4)]
    quarter = jnp.stack([second] + [swap(second, m) for m in far])
    across = swap(quarter, 2)
    pieces = [quarter, across, swap(quarter, 1), swap(across, 1)]
    own = lax.axis_index("ep")[None].astype(jnp.int32)
    weights = (
        dense_gate, dense_up, expert_gate[0], expert_up[0], dense_down, expert_down[0],
    )
    count = size // 4
    near_a, near_b, other = feed_forward(
        own, branch_gate, pieces, top, weights, (count, count, 2 * count)
    )
    arrived = swap(other, 1)
    back = swap(wide_sum(near_b, arrived[count:]).astype(jnp.bfloat16), 2)
    quarter = wide_sum(near_a, arrived[:count], back)
    sent = quarter.astype(jnp.bfloat16)
    returned = [swap(sent[k], 4 * k) for k in range(1, count)]
    return wide_sum(residual + quarter[0], *returned).astype(jnp.bfloat16)


def solution(mesh):
    rows = P(("grp", "ep"), None)
    deep = P(("grp", "ep"), None, None)
    experts = P("ep", None, None)
    return jax.shard_map(
        body,
        mesh=mesh,
        in_specs=(
            rows, P(), P(), P(), P(), P(), P(), P(), deep, deep, deep, P(("grp", "ep")),
            P(), P(), P(None, "ep"), P(None, "ep"), P("ep", None),
            experts, experts, experts, rows, rows,
        ),
        out_specs=rows,
        check_vma=False,
    )
```

time: 154 us -> 80.5 us (0.52)
  waiting for transfers between devices: 80.4 us -> 27.6 us
  matrix products: 29.5 us -> 0 us
  between operations: 13.6 us -> 0.08 us
  Pallas kernels: 0 us -> 13.5 us
  local copies, waits for them, and re-layouts: 13.8 us -> 23.3 us
  other arithmetic: 4.46 us -> 2.34 us
  starting transfers between devices: 11.2 us -> 12.9 us
    reduce_scatter x1 -> x0, waiting for transfers between devices: 33.4 us -> none  [body(): lax.psum_scatter(jnp.dot(dense_hidden, dense_down, preferred_element_type...]
    all_gather x1 -> x0, waiting for transfers between devices: 32.8 us -> none  [body(): lax.all_gather(second, 'ep', axis=0, tiled=True)]
    dot_general x15 -> x0, matrix products: 29.5 us -> none  [the longest x1 4.14 us: body(): jnp.dot(dense_hidden, dense_down, preferred_element_type=jnp.float32)]
    ppermute x0 -> x11, waiting for transfers between devices: none -> 27.6 us  [swap(): return lax.ppermute(block, 'ep', [(i, i ^ mask) for i in range(size)])]
    all_to_all x2 -> x0, waiting for transfers between devices: 14.1 us -> none  [the longest x1 14.1 us: body(): lax.all_to_all(answer.reshape(arrived_shape), 'ep', split_axis=1, concat_...]
    pallas_call x0 -> x2, Pallas kernels: none -> 13.5 us  [the longest x1 8.22 us: attention(): pl.pallas_call(attention_kernel, out_shape=(jax.ShapeDtypeStruct((rows, w...]
    ppermute x0 -> x11, starting transfers between devices: none -> 12.9 us  [swap(): return lax.ppermute(block, 'ep', [(i, i ^ mask) for i in range(size)])]
    all_to_all x2 -> x0, starting transfers between devices: 11.1 us -> none  [the longest x1 7.41 us: body(): lax.all_to_all(outgoing, 'ep', split_axis=0, concat_axis=1, tiled=True)]
  transfers between devices with their start and end apart: 4 -> 11, of which waited for: 3 -> 9; matrix products, arithmetic and copies ran while one was open for 9% -> 0% of each run, Pallas kernels for 0% -> 0%
where the time goes in v1:
time: 80.5 us; the launch traced here: 79.7 us
  waiting for transfers between devices  27.6 us (34%)
  local copies, waits for them, and re-layouts  23.3 us (29%)
  Pallas kernels  13.5 us (17%)
  starting transfers between devices  12.9 us (16%)
  other arithmetic  2.34 us (3%)
    ppermute x11, waiting for transfers between devices, swap(): return lax.ppermute(block, 'ep', [(i, i ^ mask) for i in range(size)])  27.6 us
    unnamed x41, local copies, waits for them, and re-layouts  23.1 us
    ppermute x11, starting transfers between devices, swap(): return lax.ppermute(block, 'ep', [(i, i ^ mask) for i in range(size)])  12.9 us
    pallas_call x1, Pallas kernels, attention(): pl.pallas_call(attention_kernel, out_shape=(jax.ShapeDtypeStruct((rows, w...  8.22 us
    pallas_call x1, Pallas kernels, feed_forward(): pl.pallas_call(kernel, out_shape=tuple((jax.ShapeDtypeStruct((c, rows, wi...  5.27 us
  transfers between devices with their start and end apart: 11, of which 9 were waited for; matrix products, arithmetic and copies ran while one was open for 0% of the time, Pallas kernels for 0%

profile of v1, /device:TPU:0, one launch (start us, length us, event | category | flops | bytes accessed | tf_op | source)
XLA Modules:
  0.0 79.7 jit_solution(13039093337403623774)
XLA Ops:
  0.0 0.7 reduce_precision.6
  0.7 0.8 copy.28
  1.4 0.7 convert_element_type.39
  2.1 0.1 copy.26
  2.2 0.1 copy.27
  2.3 0.1 fusion.12.meta_ref
  2.4 0.0 copy-start
  2.4 2.2 %copy-done = bf16[2048,1024]{1,0:T(8,128)(2,1)S(1)} copy-done((bf16[2048,1024]{1,0:T(8,128)(2,1)S(1)}, bf16[2048,1024]{1,0:T(8,128)(2,1)}, u32[]{:S(2)}) %copy-start) | copy-done | bytes 4194328
  4.6 0.0 copy-start.1
  4.6 2.2 %copy-done.1 = bf16[1024,2048]{1,0:T(8,128)(2,1)S(1)} copy-done((bf16[1024,2048]{1,0:T(8,128)(2,1)S(1)}, bf16[1024,2048]{1,0:T(8,128)(2,1)}, u32[]{:S(2)}) %copy-start.1) | copy-done | bytes 4194328
  6.8 0.0 copy-start.2
  6.8 2.2 %copy-done.2 = bf16[16,1024,128]{2,1,0:T(8,128)(2,1)S(1)} copy-done((bf16[16,1024,128]{2,1,0:T(8,128)(2,1)S(1)}, bf16[16,1024,128]{2,1,0:T(8,128)(2,1)}, u32[]{:S(2)}) %copy-start.2) | copy-done | bytes 4194328
  9.0 0.0 copy-start.3
  9.0 2.2 %copy-done.3 = bf16[16,1024,128]{2,1,0:T(8,128)(2,1)S(1)} copy-done((bf16[16,1024,128]{2,1,0:T(8,128)(2,1)S(1)}, bf16[16,1024,128]{2,1,0:T(8,128)(2,1)}, u32[]{:S(2)}) %copy-start.3) | copy-done | bytes 4194328
  11.2 0.0 copy-start.10
  11.2 1.0 %copy-done.10 = bf16[2048,128]{1,0:T(8,128)(2,1)S(1)} copy-done((bf16[2048,128]{1,0:T(8,128)(2,1)S(1)}, bf16[2048,128]{1,0:T(8,128)(2,1)}, u32[]{:S(2)}) %copy-start.10) | copy-done | bytes 524312
  12.2 0.0 copy-start.11
  12.2 1.0 %copy-done.11 = bf16[2048,128]{1,0:T(8,128)(2,1)S(1)} copy-done((bf16[2048,128]{1,0:T(8,128)(2,1)S(1)}, bf16[2048,128]{1,0:T(8,128)(2,1)}, u32[]{:S(2)}) %copy-start.11) | copy-done | bytes 524312
  13.2 0.0 copy-start.12
  13.2 0.9 %copy-done.12 = f32[16,2,1024]{2,1,0:T(2,128)S(1)} copy-done((f32[16,2,1024]{2,1,0:T(2,128)S(1)}, f32[16,2,1024]{2,1,0:T(2,128)}, u32[]{:S(2)}) %copy-start.12) | copy-done | bytes 131096
  14.1 0.0 copy-start.13
  14.1 0.8 %copy-done.13 = bf16[16,2048]{1,0:T(8,128)(2,1)S(1)} copy-done((bf16[16,2048]{1,0:T(8,128)(2,1)S(1)}, bf16[16,2048]{1,0:T(8,128)(2,1)}, u32[]{:S(2)}) %copy-start.13) | copy-done | bytes 65560
  15.0 0.0 copy-start.14
  15.0 0.7 copy-done.14
  15.7 0.0 copy-start.15
  15.7 0.7 copy-done.15
  16.4 0.0 copy-start.16
  16.4 0.7 copy-done.16
  17.1 0.7 copy-done.18
  17.7 0.7 copy-done.19
  18.4 8.2 %attention.1 = (f32[16,2048]{1,0:T(8,128)S(1)}, bf16[16,2176]{1,0:T(8,128)(2,1)S(1)}) custom-call(s32[16]{0:T(128)S(1)} %copy-done.18, f32[2]{0:T(128)S(1)} %copy-done.19, bf16[16,2048]{1,0:T(8,128)(2,1)S(1)} %copy-done.13, f32[1,2048]{1,0:T(1,128)S(1)} %bitcast.34, bf16[2,2048]{1,0:T(2,128)(2,1)S(1)} %bitcast.35, f32[1,2048]{1,0:T(1,128)S(1)} %bitcast.36, ...), custom_call_target="tpu_custom_call" | custom-call | tf_op jit(solution)/shard_map/attention/pallas_call | solution.py:155
  26.6 5.1 %collective-permute-start.2 = (bf16[16,2176]{1,0:T(8,128)(2,1)S(1)}, bf16[16,2176]{1,0:T(8,128)(2,1)S(1)}, u32[]{:S(2)}, u32[]{:S(2)}) collective-permute-start(bf16[16,2176]{1,0:T(8,128)(2,1)S(1)} %get-tuple-element.11), channel_id=1, source_target_pairs={{0,12},{1,13},{2,14},{3,15},{4,8},{5,9},{6,10},{7,11},{8,4},{9,5},... | collective-permute-start | bytes 208904 | tf_op jit(solution)/shard_map/ppermute | solution.py:261
  31.8 0.0 collective-permute-start.1
  31.8 0.6 collective-permute-start
  32.4 1.9 %collective-permute-done.2 = bf16[16,2176]{1,0:T(8,128)(2,1)S(1)} collective-permute-done((bf16[16,2176]{1,0:T(8,128)(2,1)S(1)}, bf16[16,2176]{1,0:T(8,128)(2,1)S(1)}, u32[]{:S(2)}, u32[]{:S(2)}) %collective-permute-start.2) | collective-permute-done | bytes 69664 | tf_op jit(solution)/shard_map/ppermute | solution.py:261
  34.3 3.3 %collective-permute-done.1 = bf16[16,2176]{1,0:T(8,128)(2,1)S(1)} collective-permute-done((bf16[16,2176]{1,0:T(8,128)(2,1)S(1)}, bf16[16,2176]{1,0:T(8,128)(2,1)S(1)}, u32[]{:S(2)}, u32[]{:S(2)}) %collective-permute-start.1) | collective-permute-done | bytes 69664 | tf_op jit(solution)/shard_map/ppermute | solution.py:261
  37.7 0.0 collective-permute-done
  37.7 1.6 %collective-permute-start.3 = (bf16[4,16,2176]{2,1,0:T(8,128)(2,1)S(1)}, bf16[4,16,2176]{2,1,0:T(8,128)(2,1)}, u32[]{:S(2)}, u32[]{:S(2)}) collective-permute-start(bf16[4,16,2176]{2,1,0:T(8,128)(2,1)S(1)} %pad_maximum_fusion.refs_2_), channel_id=1, source_target_pairs={{0,2},{1,3},{2,0},{3,1},{4,6},{5,7},{6,4},{7,5},{8,10},{9,11},{10,... | collective-permute-start | bytes 835592 | tf_op jit(solution)/shard_map/ppermute | solution.py:261
  39.3 0.0 collective-permute-start.4
  39.3 6.6 %collective-permute-done.3.refs_3_ = bf16[4,16,2176]{2,1,0:T(8,128)(2,1)} collective-permute-done((bf16[4,16,2176]{2,1,0:T(8,128)(2,1)S(1)}, bf16[4,16,2176]{2,1,0:T(8,128)(2,1)}, u32[]{:S(2)}, u32[]{:S(2)}) %collective-permute-start.3) | collective-permute-done | bytes 278560 | tf_op jit(solution)/shard_map/ppermute | solution.py:261
  45.9 0.0 collective-permute-start.5
  45.9 0.0 collective-permute-done.4.refs_4_
  45.9 1.9 %collective-permute-done.5.refs_5_ = bf16[4,16,2176]{2,1,0:T(8,128)(2,1)} collective-permute-done((bf16[4,16,2176]{2,1,0:T(8,128)(2,1)}, bf16[4,16,2176]{2,1,0:T(8,128)(2,1)}, u32[]{:S(2)}, u32[]{:S(2)}) %collective-permute-start.5) | collective-permute-done | bytes 278560 | tf_op jit(solution)/shard_map/ppermute | solution.py:261
  47.8 0.0 copy-done.4
  47.8 0.0 copy-done.7
  47.9 1.6 %copy-done.5 = bf16[1,2048,512]{2,1,0:T(8,128)(2,1)S(1)} copy-done((bf16[1,2048,512]{2,1,0:T(8,128)(2,1)S(1)}, bf16[1,2048,512]{2,1,0:T(8,128)(2,1)}, u32[]{:S(2)}) %copy-start.5) | copy-done | bytes 2097176
  49.4 1.6 %copy-done.6 = bf16[1,512,2048]{2,1,0:T(8,128)(2,1)S(1)} copy-done((bf16[1,512,2048]{2,1,0:T(8,128)(2,1)S(1)}, bf16[1,512,2048]{2,1,0:T(8,128)(2,1)}, u32[]{:S(2)}) %copy-start.6) | copy-done | bytes 2097176
  51.0 1.2 %copy-done.8 = bf16[2048,256]{1,0:T(8,128)(2,1)S(1)} copy-done((bf16[2048,256]{1,0:T(8,128)(2,1)S(1)}, bf16[2048,256]{1,0:T(8,128)(2,1)}, u32[]{:S(2)}) %copy-start.8) | copy-done | bytes 1048600
  52.3 1.2 %copy-done.9 = bf16[256,2048]{1,0:T(8,128)(2,1)S(1)} copy-done((bf16[256,2048]{1,0:T(8,128)(2,1)S(1)}, bf16[256,2048]{1,0:T(8,128)(2,1)}, u32[]{:S(2)}) %copy-start.9) | copy-done | bytes 1048600
  53.5 0.7 copy-done.17
  54.2 5.3 %feed_forward.1 = (bf16[4,16,2048]{2,1,0:T(8,128)(2,1)S(1)}, bf16[4,16,2048]{2,1,0:T(8,128)(2,1)S(1)}, bf16[8,16,2048]{2,1,0:T(8,128)(2,1)S(1)}) custom-call(s32[1]{0:T(128)} %bitcast.3.refs_0_, f32[1,2048]{1,0:T(1,128)S(1)} %bitcast.37, bf16[4,16,2176]{2,1,0:T(8,128)(2,1)S(1)} %pad_maximum_fusion.refs_2_, ...), custom_call_target="tpu_custom_call" | custom-call | tf_op jit(solution)/shard_map/feed_forward/pallas_call | solution.py:245
  59.5 0.2 collective-permute-start.6
  59.7 1.8 %collective-permute-done.6 = bf16[8,16,2048]{2,1,0:T(8,128)(2,1)S(1)} collective-permute-done((bf16[8,16,2048]{2,1,0:T(8,128)(2,1)S(1)}, bf16[8,16,2048]{2,1,0:T(8,128)(2,1)S(1)}, u32[]{:S(2)}, u32[]{:S(2)}) %collective-permute-start.6) | collective-permute-done | bytes 524320 | tf_op jit(solution)/shard_map/ppermute | solution.py:261
  61.4 0.1 add_convert_fusion
  61.5 1.8 %collective-permute-start.7 = (bf16[4,16,2048]{2,1,0:T(8,128)(2,1)S(1)}, bf16[4,16,2048]{2,1,0:T(8,128)(2,1)S(1)}, u32[]{:S(2)}, u32[]{:S(2)}) collective-permute-start(bf16[4,16,2048]{2,1,0:T(8,128)(2,1)S(1)} %add_convert_fusion), channel_id=1, source_target_pairs={{0,2},{1,3},{2,0},{3,1},{4,6},{5,7},{6,4},{7,5},{8,10},{9,11},{10,... | collective-permute-start | bytes 786440 | tf_op jit(solution)/shard_map/ppermute | solution.py:261
  63.3 6.6 %collective-permute-done.7 = bf16[4,16,2048]{2,1,0:T(8,128)(2,1)S(1)} collective-permute-done((bf16[4,16,2048]{2,1,0:T(8,128)(2,1)S(1)}, bf16[4,16,2048]{2,1,0:T(8,128)(2,1)S(1)}, u32[]{:S(2)}, u32[]{:S(2)}) %collective-permute-start.7) | collective-permute-done | bytes 262176 | tf_op jit(solution)/shard_map/ppermute | solution.py:261
  69.9 0.1 fusion.13
  70.0 0.4 collective-permute-start.8
  70.4 1.5 %collective-permute-start.10 = (bf16[16,2048]{1,0:T(8,128)(2,1)S(1)}, bf16[16,2048]{1,0:T(8,128)(2,1)S(1)}, u32[]{:S(2)}, u32[]{:S(2)}) collective-permute-start(bf16[16,2048]{1,0:T(8,128)(2,1)S(1)} %get-tuple-element.18), channel_id=1, source_target_pairs={{0,12},{1,13},{2,14},{3,15},{4,8},{5,9},{6,10},{7,11},{8,4},{9,5},... | collective-permute-start | bytes 196616 | tf_op jit(solution)/shard_map/ppermute | solution.py:261
  71.9 1.7 %collective-permute-start.9 = (bf16[16,2048]{1,0:T(8,128)(2,1)S(1)}, bf16[16,2048]{1,0:T(8,128)(2,1)S(1)}, u32[]{:S(2)}, u32[]{:S(2)}) collective-permute-start(bf16[16,2048]{1,0:T(8,128)(2,1)S(1)} %get-tuple-element.19), channel_id=1, source_target_pairs={{0,8},{1,9},{2,10},{3,11},{4,12},{5,13},{6,14},{7,15},{8,0},{9,1},... | collective-permute-start | bytes 196616 | tf_op jit(solution)/shard_map/ppermute | solution.py:261
  73.6 1.5 %collective-permute-done.8 = bf16[16,2048]{1,0:T(8,128)(2,1)S(1)} collective-permute-done((bf16[16,2048]{1,0:T(8,128)(2,1)S(1)}, bf16[16,2048]{1,0:T(8,128)(2,1)S(1)}, u32[]{:S(2)}, u32[]{:S(2)}) %collective-permute-start.8) | collective-permute-done | bytes 65568 | tf_op jit(solution)/shard_map/ppermute | solution.py:261
  75.2 1.3 %collective-permute-done.10 = bf16[16,2048]{1,0:T(8,128)(2,1)S(1)} collective-permute-done((bf16[16,2048]{1,0:T(8,128)(2,1)S(1)}, bf16[16,2048]{1,0:T(8,128)(2,1)S(1)}, u32[]{:S(2)}, u32[]{:S(2)}) %collective-permute-start.10) | collective-permute-done | bytes 65568 | tf_op jit(solution)/shard_map/ppermute | solution.py:261
  76.5 2.5 %collective-permute-done.9 = bf16[16,2048]{1,0:T(8,128)(2,1)S(1)} collective-permute-done((bf16[16,2048]{1,0:T(8,128)(2,1)S(1)}, bf16[16,2048]{1,0:T(8,128)(2,1)S(1)}, u32[]{:S(2)}, u32[]{:S(2)}) %collective-permute-start.9) | collective-permute-done | bytes 65568 | tf_op jit(solution)/shard_map/ppermute | solution.py:261
  79.0 0.7 fusion.4
  (12 shorter events, 0.1 us)
Async XLA Ops:
  2.4 2.2 %copy-start = (bf16[2048,1024]{1,0:T(8,128)(2,1)S(1)}, bf16[2048,1024]{1,0:T(8,128)(2,1)}, u32[]{:S(2)}) copy-start(bf16[2048,1024]{1,0:T(8,128)(2,1)} %wq_hbm.1) | copy-start | bytes 12582916
  4.6 2.2 %copy-start.1 = (bf16[1024,2048]{1,0:T(8,128)(2,1)S(1)}, bf16[1024,2048]{1,0:T(8,128)(2,1)}, u32[]{:S(2)}) copy-start(bf16[1024,2048]{1,0:T(8,128)(2,1)} %wo_hbm.1) | copy-start | bytes 12582916
  6.8 2.2 %copy-start.2 = (bf16[16,1024,128]{2,1,0:T(8,128)(2,1)S(1)}, bf16[16,1024,128]{2,1,0:T(8,128)(2,1)}, u32[]{:S(2)}) copy-start(bf16[16,1024,128]{2,1,0:T(8,128)(2,1)} %keys_hbm.1) | copy-start | bytes 12582916
  9.0 2.2 %copy-start.3 = (bf16[16,1024,128]{2,1,0:T(8,128)(2,1)S(1)}, bf16[16,1024,128]{2,1,0:T(8,128)(2,1)}, u32[]{:S(2)}) copy-start(bf16[16,1024,128]{2,1,0:T(8,128)(2,1)} %values_hbm.1) | copy-start | bytes 12582916
  11.2 1.0 %copy-start.10 = (bf16[2048,128]{1,0:T(8,128)(2,1)S(1)}, bf16[2048,128]{1,0:T(8,128)(2,1)}, u32[]{:S(2)}) copy-start(bf16[2048,128]{1,0:T(8,128)(2,1)} %wk_hbm.1) | copy-start | bytes 1572868
  12.2 1.0 %copy-start.11 = (bf16[2048,128]{1,0:T(8,128)(2,1)S(1)}, bf16[2048,128]{1,0:T(8,128)(2,1)}, u32[]{:S(2)}) copy-start(bf16[2048,128]{1,0:T(8,128)(2,1)} %wv_hbm.1) | copy-start | bytes 1572868
  13.2 0.9 %copy-start.12 = (f32[16,2,1024]{2,1,0:T(2,128)S(1)}, f32[16,2,1024]{2,1,0:T(2,128)}, u32[]{:S(2)}) copy-start(f32[16,2,1024]{2,1,0:T(2,128)} %logsum_hbm.1) | copy-start | bytes 393220
  14.1 0.8 %copy-start.13 = (bf16[16,2048]{1,0:T(8,128)(2,1)S(1)}, bf16[16,2048]{1,0:T(8,128)(2,1)}, u32[]{:S(2)}) copy-start(bf16[16,2048]{1,0:T(8,128)(2,1)} %tokens_ref.1) | copy-start | bytes 196612
  15.0 0.7 copy-start.14
  15.7 0.7 copy-start.15
  16.4 0.7 copy-start.16
  17.1 0.7 copy-start.18
  17.7 0.7 copy-start.19
  18.4 29.5 %copy-start.4 = (bf16[1,2048,512]{2,1,0:T(8,128)(2,1)S(1)}, bf16[1,2048,512]{2,1,0:T(8,128)(2,1)}, u32[]{:S(2)}) copy-start(bf16[1,2048,512]{2,1,0:T(8,128)(2,1)} %param.39) | copy-start | bytes 6291460
  18.4 29.5 %copy-start.7 = (bf16[2048,256]{1,0:T(8,128)(2,1)S(1)}, bf16[2048,256]{1,0:T(8,128)(2,1)}, u32[]{:S(2)}) copy-start(bf16[2048,256]{1,0:T(8,128)(2,1)} %refs_6_.1) | copy-start | bytes 3145732
  26.6 7.7 %collective-permute-start.2 = (bf16[16,2176]{1,0:T(8,128)(2,1)S(1)}, bf16[16,2176]{1,0:T(8,128)(2,1)S(1)}, u32[]{:S(2)}, u32[]{:S(2)}) collective-permute-start(bf16[16,2176]{1,0:T(8,128)(2,1)S(1)} %get-tuple-element.11), channel_id=1, source_target_pairs={{0,12},{1,13},{2,14},{3,15},{4,8},{5,9},{6,10},{7,11},{8,4},{9,5},... | collective-permute-start | bytes 208904 | tf_op jit(solution)/shard_map/ppermute | solution.py:261
  31.8 5.9 %collective-permute-start.1 = (bf16[16,2176]{1,0:T(8,128)(2,1)S(1)}, bf16[16,2176]{1,0:T(8,128)(2,1)S(1)}, u32[]{:S(2)}, u32[]{:S(2)}) collective-permute-start(bf16[16,2176]{1,0:T(8,128)(2,1)S(1)} %get-tuple-element.11), channel_id=1, source_target_pairs={{0,8},{1,9},{2,10},{3,11},{4,12},{5,13},{6,14},{7,15},{8,0},{9,1},... | collective-permute-start | bytes 208904 | tf_op jit(solution)/shard_map/ppermute | solution.py:261
  31.8 5.9 %collective-permute-start = (bf16[16,2176]{1,0:T(8,128)(2,1)S(1)}, bf16[16,2176]{1,0:T(8,128)(2,1)S(1)}, u32[]{:S(2)}, u32[]{:S(2)}) collective-permute-start(bf16[16,2176]{1,0:T(8,128)(2,1)S(1)} %get-tuple-element.11), channel_id=1, source_target_pairs={{0,4},{1,5},{2,6},{3,7},{4,0},{5,1},{6,2},{7,3},{8,12},{9,13},{10,... | collective-permute-start | bytes 208904 | tf_op jit(solution)/shard_map/ppermute | solution.py:261
  37.7 8.2 %collective-permute-start.3 = (bf16[4,16,2176]{2,1,0:T(8,128)(2,1)S(1)}, bf16[4,16,2176]{2,1,0:T(8,128)(2,1)}, u32[]{:S(2)}, u32[]{:S(2)}) collective-permute-start(bf16[4,16,2176]{2,1,0:T(8,128)(2,1)S(1)} %pad_maximum_fusion.refs_2_), channel_id=1, source_target_pairs={{0,2},{1,3},{2,0},{3,1},{4,6},{5,7},{6,4},{7,5},{8,10},{9,11},{10,... | collective-permute-start | bytes 835592 | tf_op jit(solution)/shard_map/ppermute | solution.py:261
  39.3 6.6 %collective-permute-start.4 = (bf16[4,16,2176]{2,1,0:T(8,128)(2,1)S(1)}, bf16[4,16,2176]{2,1,0:T(8,128)(2,1)}, u32[]{:S(2)}, u32[]{:S(2)}) collective-permute-start(bf16[4,16,2176]{2,1,0:T(8,128)(2,1)S(1)} %pad_maximum_fusion.refs_2_), channel_id=1, source_target_pairs={{0,1},{1,0},{2,3},{3,2},{4,5},{5,4},{6,7},{7,6},{8,9},{9,8},{10,11... | collective-permute-start | bytes 835592 | tf_op jit(solution)/shard_map/ppermute | solution.py:261
  45.9 1.9 %collective-permute-start.5 = (bf16[4,16,2176]{2,1,0:T(8,128)(2,1)}, bf16[4,16,2176]{2,1,0:T(8,128)(2,1)}, u32[]{:S(2)}, u32[]{:S(2)}) collective-permute-start(bf16[4,16,2176]{2,1,0:T(8,128)(2,1)} %collective-permute-done.3.refs_3_), channel_id=1, source_target_pairs={{0,1},{1,0},{2,3},{3,2},{4,5},{5,4},{6,7},{7,6},{8,9},{9,8},{10,11... | collective-permute-start | bytes 835592 | tf_op jit(solution)/shard_map/ppermute | solution.py:261
  47.9 1.6 %copy-start.5 = (bf16[1,2048,512]{2,1,0:T(8,128)(2,1)S(1)}, bf16[1,2048,512]{2,1,0:T(8,128)(2,1)}, u32[]{:S(2)}) copy-start(bf16[1,2048,512]{2,1,0:T(8,128)(2,1)} %param.40) | copy-start | bytes 6291460
  49.4 1.6 %copy-start.6 = (bf16[1,512,2048]{2,1,0:T(8,128)(2,1)S(1)}, bf16[1,512,2048]{2,1,0:T(8,128)(2,1)}, u32[]{:S(2)}) copy-start(bf16[1,512,2048]{2,1,0:T(8,128)(2,1)} %param.41) | copy-start | bytes 6291460
  51.0 1.2 %copy-start.8 = (bf16[2048,256]{1,0:T(8,128)(2,1)S(1)}, bf16[2048,256]{1,0:T(8,128)(2,1)}, u32[]{:S(2)}) copy-start(bf16[2048,256]{1,0:T(8,128)(2,1)} %refs_7_.1) | copy-start | bytes 3145732
  52.3 1.2 %copy-start.9 = (bf16[256,2048]{1,0:T(8,128)(2,1)S(1)}, bf16[256,2048]{1,0:T(8,128)(2,1)}, u32[]{:S(2)}) copy-start(bf16[256,2048]{1,0:T(8,128)(2,1)} %refs_10_.1) | copy-start | bytes 3145732
  53.5 0.7 copy-start.17
  59.5 2.0 %collective-permute-start.6 = (bf16[8,16,2048]{2,1,0:T(8,128)(2,1)S(1)}, bf16[8,16,2048]{2,1,0:T(8,128)(2,1)S(1)}, u32[]{:S(2)}, u32[]{:S(2)}) collective-permute-start(bf16[8,16,2048]{2,1,0:T(8,128)(2,1)S(1)} %get-tuple-element.13), channel_id=1, source_target_pairs={{0,1},{1,0},{2,3},{3,2},{4,5},{5,4},{6,7},{7,6},{8,9},{9,8},{10,11... | collective-permute-start | bytes 1572872 | tf_op jit(solution)/shard_map/ppermute | solution.py:261
  61.5 8.4 %collective-permute-start.7 = (bf16[4,16,2048]{2,1,0:T(8,128)(2,1)S(1)}, bf16[4,16,2048]{2,1,0:T(8,128)(2,1)S(1)}, u32[]{:S(2)}, u32[]{:S(2)}) collective-permute-start(bf16[4,16,2048]{2,1,0:T(8,128)(2,1)S(1)} %add_convert_fusion), channel_id=1, source_target_pairs={{0,2},{1,3},{2,0},{3,1},{4,6},{5,7},{6,4},{7,5},{8,10},{9,11},{10,... | collective-permute-start | bytes 786440 | tf_op jit(solution)/shard_map/ppermute | solution.py:261
  70.0 5.1 %collective-permute-start.8 = (bf16[16,2048]{1,0:T(8,128)(2,1)S(1)}, bf16[16,2048]{1,0:T(8,128)(2,1)S(1)}, u32[]{:S(2)}, u32[]{:S(2)}) collective-permute-start(bf16[16,2048]{1,0:T(8,128)(2,1)S(1)} %get-tuple-element.17), channel_id=1, source_target_pairs={{0,4},{1,5},{2,6},{3,7},{4,0},{5,1},{6,2},{7,3},{8,12},{9,13},{10,... | collective-permute-start | bytes 196616 | tf_op jit(solution)/shard_map/ppermute | solution.py:261
  70.4 6.1 %collective-permute-start.10 = (bf16[16,2048]{1,0:T(8,128)(2,1)S(1)}, bf16[16,2048]{1,0:T(8,128)(2,1)S(1)}, u32[]{:S(2)}, u32[]{:S(2)}) collective-permute-start(bf16[16,2048]{1,0:T(8,128)(2,1)S(1)} %get-tuple-element.18), channel_id=1, source_target_pairs={{0,12},{1,13},{2,14},{3,15},{4,8},{5,9},{6,10},{7,11},{8,4},{9,5},... | collective-permute-start | bytes 196616 | tf_op jit(solution)/shard_map/ppermute | solution.py:261
  71.9 7.1 %collective-permute-start.9 = (bf16[16,2048]{1,0:T(8,128)(2,1)S(1)}, bf16[16,2048]{1,0:T(8,128)(2,1)S(1)}, u32[]{:S(2)}, u32[]{:S(2)}) collective-permute-start(bf16[16,2048]{1,0:T(8,128)(2,1)S(1)} %get-tuple-element.19), channel_id=1, source_target_pairs={{0,8},{1,9},{2,10},{3,11},{4,12},{5,13},{6,14},{7,15},{8,0},{9,1},... | collective-permute-start | bytes 196616 | tf_op jit(solution)/shard_map/ppermute | solution.py:261

commit v2 on v1

--- a/solution.py
+++ b/solution.py
@@ -12,6 +12,10 @@
 NT = (((1,), (1,)), ((), ()))
 
 
+def in_hbm(array):
+    return pltpu.with_memory_space_constraint(array, pltpu.HBM)
+
+
 def mm(a, b):
     return jnp.dot(a, b, preferred_element_type=jnp.float32)
 
@@ -21,12 +25,16 @@
     return (scaled * gain).astype(jnp.bfloat16)
 
 
-def attention_kernel(
-    lengths_ref, bias_ref, tokens_ref, attn_gain_ref, forget_ref, ffn_gain_ref, meta_ref,
-    wq_hbm, wk_hbm, wv_hbm, wo_hbm, keys_hbm, values_hbm, logsum_hbm,
-    residual_ref, second_ref,
-    wq, wk, wv, wo, keys, values, logsum, masked_q, attended, weight_sems, cache_sems,
-):
+def attention_kernel(*refs):
+    sources = refs[:15]
+    residual_ref, second_ref = refs[15:17]
+    scratch = refs[17:]
+    (
+        tokens_ref, attn_gain_ref, forget_ref, lengths_ref, bias_ref, routes_ref, shares_ref,
+        ffn_gain_ref, wq, wk, wv, wo, logsum, keys, values,
+        masked_q, attended, weight_sems, cache_sems,
+    ) = scratch
+    keys_hbm, values_hbm = sources[13:]
     rows, width = tokens_ref.shape
     kv_heads, span = logsum.shape[1], logsum.shape[2]
     kv_width = wk.shape[1]
@@ -36,10 +44,7 @@
     shift = head_size.bit_length() - 1
     scaling = 1.0 / math.sqrt(head_size)
     loads = [
-        pltpu.make_async_copy(s, d, weight_sems.at[i])
-        for i, (s, d) in enumerate(
-            ((wq_hbm, wq), (wk_hbm, wk), (wv_hbm, wv), (logsum_hbm, logsum), (wo_hbm, wo))
-        )
+        pltpu.make_async_copy(sources[i], scratch[i], weight_sems.at[i]) for i in range(13)
     ]
     key_loads = [
         pltpu.make_async_copy(keys_hbm.at[b], keys.at[b], cache_sems.at[0, b]) for b in range(rows)
@@ -48,12 +53,30 @@
         pltpu.make_async_copy(values_hbm.at[b], values.at[b], cache_sems.at[1, b])
         for b in range(rows)
     ]
-    for load in loads[:4]:
+    for load in loads[:11] + loads[12:]:
         load.start()
     for b in range(rows):
         key_loads[b].start()
         value_loads[b].start()
-    loads[4].start()
+    loads[11].start()
+    for load in loads[:8]:
+        load.wait()
+
+    meta_row = lax.broadcasted_iota(jnp.int32, (rows, rows), 0)
+    meta_lane = lax.broadcasted_iota(jnp.int32, (rows, rows), 1)
+    meta_column = lax.broadcasted_iota(jnp.int32, (rows, META), 1)
+    meta = jnp.zeros((rows, META), jnp.float32)
+    top = routes_ref.shape[0]
+    for k in range(top):
+        share = shares_ref[k : k + 1, :]
+        high = share.astype(jnp.bfloat16).astype(jnp.float32)
+        middle = (share - high).astype(jnp.bfloat16).astype(jnp.float32)
+        low = share - high - middle
+        route = routes_ref[k : k + 1, :].astype(jnp.float32)
+        for part, value in enumerate((route, high, middle, low)):
+            column = jnp.sum(jnp.where(meta_row == meta_lane, value, 0.0), axis=1, keepdims=True)
+            meta = jnp.where(meta_column == part * top + k, column, meta)
+    second_ref[:, width:] = meta.astype(jnp.bfloat16)
 
     tokens = tokens_ref[...].astype(jnp.float32)
     normed = norm_block(tokens, attn_gain_ref[...])
@@ -75,7 +98,7 @@
     )
     fold = (fold_lane == fold_target).astype(jnp.float32).astype(jnp.bfloat16)
 
-    loads[0].wait()
+    loads[8].wait()
     queries = mm(normed, wq[...]).astype(jnp.bfloat16).astype(jnp.float32) * scaling
     for b in range(rows):
         masked_q[b * heads : (b + 1) * heads, :] = jnp.where(
@@ -83,11 +106,11 @@
         ).astype(jnp.bfloat16)
     spread_q = mm(masked_q[...], fold)
     spread_q16 = spread_q.astype(jnp.bfloat16)
-    loads[1].wait()
+    loads[9].wait()
     new_keys = mm(normed, wk[...]).astype(jnp.bfloat16).astype(jnp.float32)
-    loads[2].wait()
+    loads[10].wait()
     new_values = mm(normed, wv[...]).astype(jnp.bfloat16).astype(jnp.float32)
-    loads[3].wait()
+    loads[12].wait()
     position = lax.broadcasted_iota(jnp.int32, (1, span), 1)
 
     step = math.gcd(rows, 4)
@@ -136,56 +159,49 @@
     wide = lax.dot_general(attended[...], fold, NT, preferred_element_type=jnp.float32)
     wide = jnp.where(own_head[None], wide.reshape(rows, heads, -1), 0.0)
     side = jnp.sum(wide, axis=1).astype(jnp.bfloat16)
-    loads[4].wait()
+    loads[11].wait()
     residual = tokens + mm(side, wo[...])
     residual_ref[...] = residual
     second_ref[:, :width] = norm_block(residual, ffn_gain_ref[...])
-    second_ref[:, width:] = meta_ref[...]
-
-
-def attention(
-    tokens, attn_gain, w_query, w_key, w_value, w_forget, forget_bias, w_attn_out,
-    cache_keys, cache_values, cache_logsum, lengths, ffn_gain, meta,
-):
+
+
+def attention(operands, heads):
+    tokens, w_query, w_key = operands[0], operands[8], operands[9]
     rows, width = tokens.shape
-    heads = w_query.shape[1] // (w_key.shape[1] // cache_logsum.shape[1])
-    smem = pl.BlockSpec(memory_space=pltpu.SMEM)
     vmem = pl.BlockSpec(memory_space=pltpu.VMEM)
-    hbm = pl.BlockSpec(memory_space=pl.ANY)
+    hbm = pl.BlockSpec(memory_space=pltpu.HBM)
+    smem = (3, 4)
     return pl.pallas_call(
         attention_kernel,
         out_shape=(
             jax.ShapeDtypeStruct((rows, width), jnp.float32),
             jax.ShapeDtypeStruct((rows, width + META), jnp.bfloat16),
         ),
-        in_specs=[smem, smem] + [vmem] * 5 + [hbm] * 7,
+        in_specs=[hbm] * len(operands),
         out_specs=(vmem, vmem),
         scratch_shapes=[
-            pltpu.VMEM(a.shape, a.dtype)
-            for a in (w_query, w_key, w_value, w_attn_out, cache_keys, cache_values, cache_logsum)
+            (pltpu.SMEM if i in smem else pltpu.VMEM)(a.shape, a.dtype)
+            for i, a in enumerate(operands)
         ]
         + [
             pltpu.VMEM((rows * heads, w_query.shape[1]), jnp.bfloat16),
             pltpu.VMEM((rows * heads, w_key.shape[1]), jnp.bfloat16),
-            pltpu.SemaphoreType.DMA((5,)),
+            pltpu.SemaphoreType.DMA((13,)),
             pltpu.SemaphoreType.DMA((2, rows)),
         ],
-        compiler_params=pltpu.CompilerParams(vmem_limit_bytes=36 << 20),
+        compiler_params=pltpu.CompilerParams(vmem_limit_bytes=30 << 20),
         name="attention",
-    )(
-        lengths, forget_bias, tokens, attn_gain[None], w_forget.T, ffn_gain[None], meta,
-        w_query, w_key, w_value, w_attn_out, cache_keys, cache_values, cache_logsum,
-    )
+    )(*map(in_hbm, operands))
 
 
 def feed_forward_kernel(top, piece_count, *refs):
-    own_ref, gate_ref = refs[:2]
+    own_ref, gate_hbm = refs[:2]
     pieces = refs[2 : 2 + piece_count]
-    sources = refs[2 + piece_count : 8 + piece_count]
-    outs = refs[8 + piece_count : -8]
-    buffers = refs[-8:-2]
+    sources = refs[2 + piece_count : 8 + piece_count] + (gate_hbm,)
+    outs = refs[8 + piece_count : -9]
+    buffers = refs[-9:-2]
+    dense_gate, dense_up, expert_gate, expert_up, dense_down, expert_down, gate_ref = buffers
     x_ref, sems = refs[-2:]
-    dense_gate, dense_up, expert_gate, expert_up, dense_down, expert_down = buffers
     loads = [
         pltpu.make_async_copy(s, d, sems.at[i]) for i, (s, d) in enumerate(zip(sources, buffers))
     ]
@@ -208,15 +224,16 @@
         jnp.where(meta[:, :top] == own, weights, 0.0), axis=1, keepdims=True
     )
     x = x_ref[...]
-    share = jax.nn.sigmoid(
-        jnp.sum(x.astype(jnp.float32) * gate_ref[...], axis=1, keepdims=True)
-    )
     loads[0].wait()
     loads[1].wait()
     hidden = (jax.nn.silu(mm(x, dense_gate[...])) * mm(x, dense_up[...])).astype(jnp.bfloat16)
     loads[2].wait()
     loads[3].wait()
     middle = (jax.nn.silu(mm(x, expert_gate[...])) * mm(x, expert_up[...])).astype(jnp.bfloat16)
+    loads[6].wait()
+    share = jax.nn.sigmoid(
+        jnp.sum(x.astype(jnp.float32) * gate_ref[...], axis=1, keepdims=True)
+    )
     loads[4].wait()
     loads[5].wait()
     chunk = math.gcd(width, 512)
@@ -237,7 +254,7 @@
     total = sum(p.shape[0] for p in pieces) * rows
     smem = pl.BlockSpec(memory_space=pltpu.SMEM)
     vmem = pl.BlockSpec(memory_space=pltpu.VMEM)
-    hbm = pl.BlockSpec(memory_space=pl.ANY)
+    hbm = pl.BlockSpec(memory_space=pltpu.HBM)
 
     def kernel(*refs):
         feed_forward_kernel(top, len(pieces), *refs)
@@ -247,13 +264,17 @@
         out_shape=tuple(
             jax.ShapeDtypeStruct((c, rows, width), jnp.bfloat16) for c in out_counts
         ),
-        in_specs=[smem, vmem] + [vmem] * len(pieces) + [hbm] * 6,
+        in_specs=[smem, hbm] + [vmem] * len(pieces) + [hbm] * len(weights),
         out_specs=(vmem,) * len(out_counts),
         scratch_shapes=[pltpu.VMEM(w.shape, w.dtype) for w in weights]
-        + [pltpu.VMEM((total, width), jnp.bfloat16), pltpu.SemaphoreType.DMA((6,))],
-        compiler_params=pltpu.CompilerParams(vmem_limit_bytes=36 << 20),
+        + [
+            pltpu.VMEM((1, width), branch_gate.dtype),
+            pltpu.VMEM((total, width), jnp.bfloat16),
+            pltpu.SemaphoreType.DMA((7,)),
+        ],
+        compiler_params=pltpu.CompilerParams(vmem_limit_bytes=30 << 20),
         name="feed_forward",
-    )(own, branch_gate[None], *pieces, *weights)
+    )(own, in_hbm(branch_gate[None]), *pieces, *map(in_hbm, weights))
 
 
 def swap(block, mask):
@@ -276,23 +297,21 @@
 ):
     size = lax.axis_size("ep")
     top = routes.shape[1]
-    high = lax.reduce_precision(route_weights, 8, 7)
-    middle = lax.reduce_precision(route_weights - high, 8, 7)
-    low = route_weights - high - middle
-    meta = jnp.concatenate([routes.astype(jnp.float32), high, middle, low], axis=1)
-    meta = jnp.pad(meta, ((0, 0), (0, META - 4 * top))).astype(jnp.bfloat16)
+    heads = w_query.shape[1] * cache_logsum.shape[1] // w_key.shape[1]
     residual, second = attention(
-        tokens, attn_gain, w_query, w_key, w_value, w_forget, forget_bias, w_attn_out,
-        cache_keys, cache_values, cache_logsum, lengths, ffn_gain, meta,
-    )
+        (
+            tokens, attn_gain[None], w_forget.T, lengths, forget_bias, routes.T,
+            route_weights.T, ffn_gain[None], w_query, w_key, w_value, w_attn_out,
+            cache_logsum, cache_keys, cache_values,
+        ),
+        heads,
+    )
+    weights = (dense_gate, dense_up, expert_gate[0], expert_up[0], dense_down, expert_down[0])
     far = [4 * k for k in range(1, size // 4)]
     quarter = jnp.stack([second] + [swap(second, m) for m in far])
     across = swap(quarter, 2)
     pieces = [quarter, across, swap(quarter, 1), swap(across, 1)]
     own = lax.axis_index("ep")[None].astype(jnp.int32)
-    weights = (
-        dense_gate, dense_up, expert_gate[0], expert_up[0], dense_down, expert_down[0],
-    )
     count = size // 4
     near_a, near_b, other = feed_forward(
         own, branch_gate, pieces, top, weights, (count, count, 2 * count)

time: 80.5 us -> 57.4 us (0.71)
  local copies, waits for them, and re-layouts: 23.3 us -> 0.02 us
  Pallas kernels: 13.5 us -> 16.2 us
  other arithmetic: 2.34 us -> 0.88 us
    unnamed x41 -> x0, local copies, waits for them, and re-layouts: 23.1 us -> none
    pallas_call x1, Pallas kernels: 8.22 us -> 10.4 us  [attention(): pl.pallas_call(attention_kernel, out_shape=(jax.ShapeDtypeStruct((rows, w...]
where the time goes in v2:
time: 57.4 us; the launch traced here: 57.2 us
  waiting for transfers between devices  27.2 us (47%)
  Pallas kernels  16.2 us (28%)
  starting transfers between devices  12.9 us (22%)
  other arithmetic  0.88 us (2%)
    ppermute x11, waiting for transfers between devices, swap(): return lax.ppermute(block, 'ep', [(i, i ^ mask) for i in range(size)])  27.2 us
    ppermute x11, starting transfers between devices, swap(): return lax.ppermute(block, 'ep', [(i, i ^ mask) for i in range(size)])  12.9 us
    pallas_call x1, Pallas kernels, attention(): pl.pallas_call(attention_kernel, out_shape=(jax.ShapeDtypeStruct((rows, w...  10.4 us
    pallas_call x1, Pallas kernels, feed_forward(): pl.pallas_call(kernel, out_shape=tuple((jax.ShapeDtypeStruct((c, rows, wi...  5.78 us
  transfers between devices with their start and end apart: 11, of which 9 were waited for; matrix products, arithmetic and copies ran while one was open for 0% of the time, Pallas kernels for 0%

profile of v2, /device:TPU:0, one launch (start us, length us, event | category | flops | bytes accessed | tf_op | source)
XLA Modules:
  0.0 57.2 jit_solution(6284714885689327923)
XLA Ops:
  0.0 10.4 %attention.1 = (f32[16,2048]{1,0:T(8,128)S(1)}, bf16[16,2176]{1,0:T(8,128)(2,1)S(1)}) custom-call(bf16[16,2048]{1,0:T(8,128)(2,1)} %refs_0_.1, f32[1,2048]{1,0:T(1,128)} %bitcast.39, bf16[2,2048]{1,0:T(2,128)(2,1)} %bitcast.40, s32[16]{0:T(128)} %refs_3_.1, f32[2]{0:T(128)} %refs_4_.1, s32[4,16]{1,0:T(4,128)} %bitcast.43, f32[4,16]{1,0:T(4,128)} %bitcast.44, ...), custom_call_target="tpu_custom_call" | custom-call | tf_op jit(solution)/shard_map/attention/pallas_call | solution.py:174
  10.4 5.1 %collective-permute-start.2 = (bf16[16,2176]{1,0:T(8,128)(2,1)S(1)}, bf16[16,2176]{1,0:T(8,128)(2,1)S(1)}, u32[]{:S(2)}, u32[]{:S(2)}) collective-permute-start(bf16[16,2176]{1,0:T(8,128)(2,1)S(1)} %get-tuple-element.11), channel_id=1, source_target_pairs={{0,12},{1,13},{2,14},{3,15},{4,8},{5,9},{6,10},{7,11},{8,4},{9,5},... | collective-permute-start | bytes 208904 | tf_op jit(solution)/shard_map/ppermute | solution.py:282
  15.6 0.0 collective-permute-start.1
  15.6 0.6 %collective-permute-start = (bf16[16,2176]{1,0:T(8,128)(2,1)S(1)}, bf16[16,2176]{1,0:T(8,128)(2,1)S(1)}, u32[]{:S(2)}, u32[]{:S(2)}) collective-permute-start(bf16[16,2176]{1,0:T(8,128)(2,1)S(1)} %get-tuple-element.11), channel_id=1, source_target_pairs={{0,4},{1,5},{2,6},{3,7},{4,0},{5,1},{6,2},{7,3},{8,12},{9,13},{10,... | collective-permute-start | bytes 208904 | tf_op jit(solution)/shard_map/ppermute | solution.py:282
  16.2 1.9 %collective-permute-done.2 = bf16[16,2176]{1,0:T(8,128)(2,1)S(1)} collective-permute-done((bf16[16,2176]{1,0:T(8,128)(2,1)S(1)}, bf16[16,2176]{1,0:T(8,128)(2,1)S(1)}, u32[]{:S(2)}, u32[]{:S(2)}) %collective-permute-start.2) | collective-permute-done | bytes 69664 | tf_op jit(solution)/shard_map/ppermute | solution.py:282
  18.1 3.3 %collective-permute-done.1 = bf16[16,2176]{1,0:T(8,128)(2,1)S(1)} collective-permute-done((bf16[16,2176]{1,0:T(8,128)(2,1)S(1)}, bf16[16,2176]{1,0:T(8,128)(2,1)S(1)}, u32[]{:S(2)}, u32[]{:S(2)}) %collective-permute-start.1) | collective-permute-done | bytes 69664 | tf_op jit(solution)/shard_map/ppermute | solution.py:282
  21.5 0.0 collective-permute-done
  21.5 1.6 %collective-permute-start.3 = (bf16[4,16,2176]{2,1,0:T(8,128)(2,1)S(1)}, bf16[4,16,2176]{2,1,0:T(8,128)(2,1)S(1)}, u32[]{:S(2)}, u32[]{:S(2)}) collective-permute-start(bf16[4,16,2176]{2,1,0:T(8,128)(2,1)S(1)} %pad_maximum_fusion.refs_2_), channel_id=1, source_target_pairs={{0,2},{1,3},{2,0},{3,1},{4,6},{5,7},{6,4},{7,5},{8,10},{9,11},{10,... | collective-permute-start | bytes 835592 | tf_op jit(solution)/shard_map/ppermute | solution.py:282
  23.1 0.0 collective-permute-start.4
  23.1 6.5 %collective-permute-done.3.refs_3_ = bf16[4,16,2176]{2,1,0:T(8,128)(2,1)S(1)} collective-permute-done((bf16[4,16,2176]{2,1,0:T(8,128)(2,1)S(1)}, bf16[4,16,2176]{2,1,0:T(8,128)(2,1)S(1)}, u32[]{:S(2)}, u32[]{:S(2)}) %collective-permute-start.3) | collective-permute-done | bytes 278560 | tf_op jit(solution)/shard_map/ppermute | solution.py:282
  29.6 0.0 collective-permute-start.5
  29.6 0.0 collective-permute-done.4.refs_4_
  29.6 1.6 %collective-permute-done.5.refs_5_ = bf16[4,16,2176]{2,1,0:T(8,128)(2,1)S(1)} collective-permute-done((bf16[4,16,2176]{2,1,0:T(8,128)(2,1)S(1)}, bf16[4,16,2176]{2,1,0:T(8,128)(2,1)S(1)}, u32[]{:S(2)}, u32[]{:S(2)}) %collective-permute-start.5) | collective-permute-done | bytes 278560 | tf_op jit(solution)/shard_map/ppermute | solution.py:282
  31.2 5.8 %feed_forward.1 = (bf16[4,16,2048]{2,1,0:T(8,128)(2,1)S(1)}, bf16[4,16,2048]{2,1,0:T(8,128)(2,1)S(1)}, bf16[8,16,2048]{2,1,0:T(8,128)(2,1)S(1)}) custom-call(s32[1]{0:T(128)} %bitcast.5.refs_0_, f32[1,2048]{1,0:T(1,128)} %bitcast.42, bf16[4,16,2176]{2,1,0:T(8,128)(2,1)S(1)} %pad_maximum_fusion.refs_2_, ...), custom_call_target="tpu_custom_call" | custom-call | tf_op jit(solution)/shard_map/feed_forward/pallas_call | solution.py:262
  37.0 0.2 collective-permute-start.6
  37.2 1.8 %collective-permute-done.6 = bf16[8,16,2048]{2,1,0:T(8,128)(2,1)S(1)} collective-permute-done((bf16[8,16,2048]{2,1,0:T(8,128)(2,1)S(1)}, bf16[8,16,2048]{2,1,0:T(8,128)(2,1)S(1)}, u32[]{:S(2)}, u32[]{:S(2)}) %collective-permute-start.6) | collective-permute-done | bytes 524320 | tf_op jit(solution)/shard_map/ppermute | solution.py:282
  39.0 0.1 add_convert_fusion
  39.0 1.8 %collective-permute-start.7 = (bf16[4,16,2048]{2,1,0:T(8,128)(2,1)S(1)}, bf16[4,16,2048]{2,1,0:T(8,128)(2,1)S(1)}, u32[]{:S(2)}, u32[]{:S(2)}) collective-permute-start(bf16[4,16,2048]{2,1,0:T(8,128)(2,1)S(1)} %add_convert_fusion), channel_id=1, source_target_pairs={{0,2},{1,3},{2,0},{3,1},{4,6},{5,7},{6,4},{7,5},{8,10},{9,11},{10,... | collective-permute-start | bytes 786440 | tf_op jit(solution)/shard_map/ppermute | solution.py:282
  40.8 6.6 %collective-permute-done.7 = bf16[4,16,2048]{2,1,0:T(8,128)(2,1)S(1)} collective-permute-done((bf16[4,16,2048]{2,1,0:T(8,128)(2,1)S(1)}, bf16[4,16,2048]{2,1,0:T(8,128)(2,1)S(1)}, u32[]{:S(2)}, u32[]{:S(2)}) %collective-permute-start.7) | collective-permute-done | bytes 262176 | tf_op jit(solution)/shard_map/ppermute | solution.py:282
  47.4 0.1 fusion.5
  47.6 0.4 collective-permute-start.8
  47.9 1.5 %collective-permute-start.10 = (bf16[16,2048]{1,0:T(8,128)(2,1)S(1)}, bf16[16,2048]{1,0:T(8,128)(2,1)S(1)}, u32[]{:S(2)}, u32[]{:S(2)}) collective-permute-start(bf16[16,2048]{1,0:T(8,128)(2,1)S(1)} %get-tuple-element.18), channel_id=1, source_target_pairs={{0,12},{1,13},{2,14},{3,15},{4,8},{5,9},{6,10},{7,11},{8,4},{9,5},... | collective-permute-start | bytes 196616 | tf_op jit(solution)/shard_map/ppermute | solution.py:282
  49.5 1.7 %collective-permute-start.9 = (bf16[16,2048]{1,0:T(8,128)(2,1)S(1)}, bf16[16,2048]{1,0:T(8,128)(2,1)S(1)}, u32[]{:S(2)}, u32[]{:S(2)}) collective-permute-start(bf16[16,2048]{1,0:T(8,128)(2,1)S(1)} %get-tuple-element.19), channel_id=1, source_target_pairs={{0,8},{1,9},{2,10},{3,11},{4,12},{5,13},{6,14},{7,15},{8,0},{9,1},... | collective-permute-start | bytes 196616 | tf_op jit(solution)/shard_map/ppermute | solution.py:282
  51.1 1.5 %collective-permute-done.8 = bf16[16,2048]{1,0:T(8,128)(2,1)S(1)} collective-permute-done((bf16[16,2048]{1,0:T(8,128)(2,1)S(1)}, bf16[16,2048]{1,0:T(8,128)(2,1)S(1)}, u32[]{:S(2)}, u32[]{:S(2)}) %collective-permute-start.8) | collective-permute-done | bytes 65568 | tf_op jit(solution)/shard_map/ppermute | solution.py:282
  52.7 1.3 %collective-permute-done.10 = bf16[16,2048]{1,0:T(8,128)(2,1)S(1)} collective-permute-done((bf16[16,2048]{1,0:T(8,128)(2,1)S(1)}, bf16[16,2048]{1,0:T(8,128)(2,1)S(1)}, u32[]{:S(2)}, u32[]{:S(2)}) %collective-permute-start.10) | collective-permute-done | bytes 65568 | tf_op jit(solution)/shard_map/ppermute | solution.py:282
  54.0 2.5 %collective-permute-done.9 = bf16[16,2048]{1,0:T(8,128)(2,1)S(1)} collective-permute-done((bf16[16,2048]{1,0:T(8,128)(2,1)S(1)}, bf16[16,2048]{1,0:T(8,128)(2,1)S(1)}, u32[]{:S(2)}, u32[]{:S(2)}) %collective-permute-start.9) | collective-permute-done | bytes 65568 | tf_op jit(solution)/shard_map/ppermute | solution.py:282
  56.5 0.7 %fusion.4 = bf16[16,2048]{1,0:T(8,128)(2,1)} fusion(f32[16,2048]{1,0:T(8,128)S(1)} %get-tuple-element.10, f32[4,16,2048]{2,1,0:T(8,128)S(1)} %get-tuple-element.16, bf16[16,2048]{1,0:T(8,128)(2,1)S(1)} %collective-permute-done.10, bf16[16,2048]{1,0:T(8,128)(2,1)S(1)} %collective-permute-done.9, bf16[16,2048]{1,0:T(8,128)(2,1)S(1)} %collective-permute-done.8), kind=kLoop, calls=%fused_computation.8 | loop fusion | flops 262144 | bytes 524288 | tf_op jit(solution)/shard_map/convert_element_type | solution.py:324
  (2 shorter events, 0.1 us)
Async XLA Ops:
  10.4 7.7 %collective-permute-start.2 = (bf16[16,2176]{1,0:T(8,128)(2,1)S(1)}, bf16[16,2176]{1,0:T(8,128)(2,1)S(1)}, u32[]{:S(2)}, u32[]{:S(2)}) collective-permute-start(bf16[16,2176]{1,0:T(8,128)(2,1)S(1)} %get-tuple-element.11), channel_id=1, source_target_pairs={{0,12},{1,13},{2,14},{3,15},{4,8},{5,9},{6,10},{7,11},{8,4},{9,5},... | collective-permute-start | bytes 208904 | tf_op jit(solution)/shard_map/ppermute | solution.py:282
  15.6 5.9 %collective-permute-start.1 = (bf16[16,2176]{1,0:T(8,128)(2,1)S(1)}, bf16[16,2176]{1,0:T(8,128)(2,1)S(1)}, u32[]{:S(2)}, u32[]{:S(2)}) collective-permute-start(bf16[16,2176]{1,0:T(8,128)(2,1)S(1)} %get-tuple-element.11), channel_id=1, source_target_pairs={{0,8},{1,9},{2,10},{3,11},{4,12},{5,13},{6,14},{7,15},{8,0},{9,1},... | collective-permute-start | bytes 208904 | tf_op jit(solution)/shard_map/ppermute | solution.py:282
  15.6 5.9 %collective-permute-start = (bf16[16,2176]{1,0:T(8,128)(2,1)S(1)}, bf16[16,2176]{1,0:T(8,128)(2,1)S(1)}, u32[]{:S(2)}, u32[]{:S(2)}) collective-permute-start(bf16[16,2176]{1,0:T(8,128)(2,1)S(1)} %get-tuple-element.11), channel_id=1, source_target_pairs={{0,4},{1,5},{2,6},{3,7},{4,0},{5,1},{6,2},{7,3},{8,12},{9,13},{10,... | collective-permute-start | bytes 208904 | tf_op jit(solution)/shard_map/ppermute | solution.py:282
  21.5 8.1 %collective-permute-start.3 = (bf16[4,16,2176]{2,1,0:T(8,128)(2,1)S(1)}, bf16[4,16,2176]{2,1,0:T(8,128)(2,1)S(1)}, u32[]{:S(2)}, u32[]{:S(2)}) collective-permute-start(bf16[4,16,2176]{2,1,0:T(8,128)(2,1)S(1)} %pad_maximum_fusion.refs_2_), channel_id=1, source_target_pairs={{0,2},{1,3},{2,0},{3,1},{4,6},{5,7},{6,4},{7,5},{8,10},{9,11},{10,... | collective-permute-start | bytes 835592 | tf_op jit(solution)/shard_map/ppermute | solution.py:282
  23.1 6.5 %collective-permute-start.4 = (bf16[4,16,2176]{2,1,0:T(8,128)(2,1)S(1)}, bf16[4,16,2176]{2,1,0:T(8,128)(2,1)S(1)}, u32[]{:S(2)}, u32[]{:S(2)}) collective-permute-start(bf16[4,16,2176]{2,1,0:T(8,128)(2,1)S(1)} %pad_maximum_fusion.refs_2_), channel_id=1, source_target_pairs={{0,1},{1,0},{2,3},{3,2},{4,5},{5,4},{6,7},{7,6},{8,9},{9,8},{10,11... | collective-permute-start | bytes 835592 | tf_op jit(solution)/shard_map/ppermute | solution.py:282
  29.6 1.6 %collective-permute-start.5 = (bf16[4,16,2176]{2,1,0:T(8,128)(2,1)S(1)}, bf16[4,16,2176]{2,1,0:T(8,128)(2,1)S(1)}, u32[]{:S(2)}, u32[]{:S(2)}) collective-permute-start(bf16[4,16,2176]{2,1,0:T(8,128)(2,1)S(1)} %collective-permute-done.3.refs_3_), channel_id=1, source_target_pairs={{0,1},{1,0},{2,3},{3,2},{4,5},{5,4},{6,7},{7,6},{8,9},{9,8},{10,11... | collective-permute-start | bytes 835592 | tf_op jit(solution)/shard_map/ppermute | solution.py:282
  37.0 2.0 %collective-permute-start.6 = (bf16[8,16,2048]{2,1,0:T(8,128)(2,1)S(1)}, bf16[8,16,2048]{2,1,0:T(8,128)(2,1)S(1)}, u32[]{:S(2)}, u32[]{:S(2)}) collective-permute-start(bf16[8,16,2048]{2,1,0:T(8,128)(2,1)S(1)} %get-tuple-element.13), channel_id=1, source_target_pairs={{0,1},{1,0},{2,3},{3,2},{4,5},{5,4},{6,7},{7,6},{8,9},{9,8},{10,11... | collective-permute-start | bytes 1572872 | tf_op jit(solution)/shard_map/ppermute | solution.py:282
  39.0 8.4 %collective-permute-start.7 = (bf16[4,16,2048]{2,1,0:T(8,128)(2,1)S(1)}, bf16[4,16,2048]{2,1,0:T(8,128)(2,1)S(1)}, u32[]{:S(2)}, u32[]{:S(2)}) collective-permute-start(bf16[4,16,2048]{2,1,0:T(8,128)(2,1)S(1)} %add_convert_fusion), channel_id=1, source_target_pairs={{0,2},{1,3},{2,0},{3,1},{4,6},{5,7},{6,4},{7,5},{8,10},{9,11},{10,... | collective-permute-start | bytes 786440 | tf_op jit(solution)/shard_map/ppermute | solution.py:282
  47.6 5.1 %collective-permute-start.8 = (bf16[16,2048]{1,0:T(8,128)(2,1)S(1)}, bf16[16,2048]{1,0:T(8,128)(2,1)S(1)}, u32[]{:S(2)}, u32[]{:S(2)}) collective-permute-start(bf16[16,2048]{1,0:T(8,128)(2,1)S(1)} %get-tuple-element.17), channel_id=1, source_target_pairs={{0,4},{1,5},{2,6},{3,7},{4,0},{5,1},{6,2},{7,3},{8,12},{9,13},{10,... | collective-permute-start | bytes 196616 | tf_op jit(solution)/shard_map/ppermute | solution.py:282
  47.9 6.1 %collective-permute-start.10 = (bf16[16,2048]{1,0:T(8,128)(2,1)S(1)}, bf16[16,2048]{1,0:T(8,128)(2,1)S(1)}, u32[]{:S(2)}, u32[]{:S(2)}) collective-permute-start(bf16[16,2048]{1,0:T(8,128)(2,1)S(1)} %get-tuple-element.18), channel_id=1, source_target_pairs={{0,12},{1,13},{2,14},{3,15},{4,8},{5,9},{6,10},{7,11},{8,4},{9,5},... | collective-permute-start | bytes 196616 | tf_op jit(solution)/shard_map/ppermute | solution.py:282
  49.5 7.1 %collective-permute-start.9 = (bf16[16,2048]{1,0:T(8,128)(2,1)S(1)}, bf16[16,2048]{1,0:T(8,128)(2,1)S(1)}, u32[]{:S(2)}, u32[]{:S(2)}) collective-permute-start(bf16[16,2048]{1,0:T(8,128)(2,1)S(1)} %get-tuple-element.19), channel_id=1, source_target_pairs={{0,8},{1,9},{2,10},{3,11},{4,12},{5,13},{6,14},{7,15},{8,0},{9,1},... | collective-permute-start | bytes 196616 | tf_op jit(solution)/shard_map/ppermute | solution.py:282

commit v3 on v2

--- a/solution.py
+++ b/solution.py
@@ -113,7 +113,7 @@
     loads[12].wait()
     position = lax.broadcasted_iota(jnp.int32, (1, span), 1)
 
-    step = math.gcd(rows, 4)
+    step = math.gcd(rows, 8)
     for first in range(0, rows, step):
         members = range(first, first + step)
         for b in members:
@@ -313,15 +313,27 @@
     pieces = [quarter, across, swap(quarter, 1), swap(across, 1)]
     own = lax.axis_index("ep")[None].astype(jnp.int32)
     count = size // 4
-    near_a, near_b, other = feed_forward(
-        own, branch_gate, pieces, top, weights, (count, count, 2 * count)
-    )
+    half = count // 2
+    spans = ((0, half), (half, count))
+    sizes = (half, count - half)
+    *near, other = feed_forward(
+        own, branch_gate, pieces, top, weights, sizes + sizes + (2 * count,)
+    )
+    near_a, near_b = near[:2], near[2:]
     arrived = swap(other, 1)
-    back = swap(wide_sum(near_b, arrived[count:]).astype(jnp.bfloat16), 2)
-    quarter = wide_sum(near_a, arrived[:count], back)
-    sent = quarter.astype(jnp.bfloat16)
-    returned = [swap(sent[k], 4 * k) for k in range(1, count)]
-    return wide_sum(residual + quarter[0], *returned).astype(jnp.bfloat16)
+    arrived_a, arrived_b = arrived[:count], arrived[count:]
+    sum_b = [
+        wide_sum(part, arrived_b[lo:hi]).astype(jnp.bfloat16)
+        for part, (lo, hi) in zip(near_b, spans)
+    ]
+    far_back = swap(sum_b[1], 2)
+    near_back = swap(sum_b[0], 2)
+    far_sum = wide_sum(near_a[1], arrived_a[half:], far_back).astype(jnp.bfloat16)
+    returned = [swap(far_sum[k - half], 4 * k) for k in range(half, count)]
+    near_sum = wide_sum(near_a[0], arrived_a[:half], near_back)
+    near_sent = near_sum.astype(jnp.bfloat16)
+    returned += [swap(near_sent[k], 4 * k) for k in range(1, half)]
+    return wide_sum(residual + near_sum[0], *returned).astype(jnp.bfloat16)
 
 
 def solution(mesh):

time: 57.4 us -> 54.2 us (0.944)
  waiting for transfers between devices: 27.2 us -> 23.7 us
  starting transfers between devices: 12.9 us -> 14.1 us
  Pallas kernels: 16.2 us -> 15.3 us
    ppermute x11 -> x12, waiting for transfers between devices: 27.2 us -> 23.7 us  [swap(): return lax.ppermute(block, 'ep', [(i, i ^ mask) for i in range(size)])]
    ppermute x11 -> x12, starting transfers between devices: 12.9 us -> 14.1 us  [swap(): return lax.ppermute(block, 'ep', [(i, i ^ mask) for i in range(size)])]
    pallas_call x1, Pallas kernels: 10.4 us -> 9.56 us  [attention(): pl.pallas_call(attention_kernel, out_shape=(jax.ShapeDtypeStruct((rows, w...]
  transfers between devices with their start and end apart: 11 -> 12, of which waited for: 9 -> 9; matrix products, arithmetic and copies ran while one was open for 0% -> 0% of each run, Pallas kernels for 0% -> 0%
where the time goes in v3:
time: 54.2 us; the launch traced here: 54 us
  waiting for transfers between devices  23.7 us (44%)
  Pallas kernels  15.3 us (28%)
  starting transfers between devices  14.1 us (26%)
  other arithmetic  0.87 us (2%)
    ppermute x12, waiting for transfers between devices, swap(): return lax.ppermute(block, 'ep', [(i, i ^ mask) for i in range(size)])  23.7 us
    ppermute x12, starting transfers between devices, swap(): return lax.ppermute(block, 'ep', [(i, i ^ mask) for i in range(size)])  14.1 us
    pallas_call x1, Pallas kernels, attention(): pl.pallas_call(attention_kernel, out_shape=(jax.ShapeDtypeStruct((rows, w...  9.56 us
    pallas_call x1, Pallas kernels, feed_forward(): pl.pallas_call(kernel, out_shape=tuple((jax.ShapeDtypeStruct((c, rows, wi...  5.77 us
  transfers between devices with their start and end apart: 12, of which 9 were waited for; matrix products, arithmetic and copies ran while one was open for 0% of the time, Pallas kernels for 0%

profile of v3, /device:TPU:0, one launch (start us, length us, event | category | flops | bytes accessed | tf_op | source)
XLA Modules:
  0.0 54.0 jit_solution(6462655348176433330)
XLA Ops:
  0.0 9.6 %attention.1 = (f32[16,2048]{1,0:T(8,128)S(1)}, bf16[16,2176]{1,0:T(8,128)(2,1)S(1)}) custom-call(bf16[16,2048]{1,0:T(8,128)(2,1)} %refs_0_.1, f32[1,2048]{1,0:T(1,128)} %bitcast.39, bf16[2,2048]{1,0:T(2,128)(2,1)} %bitcast.40, s32[16]{0:T(128)} %refs_3_.1, f32[2]{0:T(128)} %refs_4_.1, s32[4,16]{1,0:T(4,128)} %bitcast.43, f32[4,16]{1,0:T(4,128)} %bitcast.44, ...), custom_call_target="tpu_custom_call" | custom-call | tf_op jit(solution)/shard_map/attention/pallas_call | solution.py:174
  9.6 5.1 %collective-permute-start.2 = (bf16[16,2176]{1,0:T(8,128)(2,1)S(1)}, bf16[16,2176]{1,0:T(8,128)(2,1)S(1)}, u32[]{:S(2)}, u32[]{:S(2)}) collective-permute-start(bf16[16,2176]{1,0:T(8,128)(2,1)S(1)} %get-tuple-element.13), channel_id=1, source_target_pairs={{0,12},{1,13},{2,14},{3,15},{4,8},{5,9},{6,10},{7,11},{8,4},{9,5},... | collective-permute-start | bytes 208904 | tf_op jit(solution)/shard_map/ppermute | solution.py:282
  14.7 0.0 collective-permute-start.1
  14.7 0.6 %collective-permute-start = (bf16[16,2176]{1,0:T(8,128)(2,1)S(1)}, bf16[16,2176]{1,0:T(8,128)(2,1)S(1)}, u32[]{:S(2)}, u32[]{:S(2)}) collective-permute-start(bf16[16,2176]{1,0:T(8,128)(2,1)S(1)} %get-tuple-element.13), channel_id=1, source_target_pairs={{0,4},{1,5},{2,6},{3,7},{4,0},{5,1},{6,2},{7,3},{8,12},{9,13},{10,... | collective-permute-start | bytes 208904 | tf_op jit(solution)/shard_map/ppermute | solution.py:282
  15.4 1.9 %collective-permute-done.2 = bf16[16,2176]{1,0:T(8,128)(2,1)S(1)} collective-permute-done((bf16[16,2176]{1,0:T(8,128)(2,1)S(1)}, bf16[16,2176]{1,0:T(8,128)(2,1)S(1)}, u32[]{:S(2)}, u32[]{:S(2)}) %collective-permute-start.2) | collective-permute-done | bytes 69664 | tf_op jit(solution)/shard_map/ppermute | solution.py:282
  17.3 3.3 %collective-permute-done.1 = bf16[16,2176]{1,0:T(8,128)(2,1)S(1)} collective-permute-done((bf16[16,2176]{1,0:T(8,128)(2,1)S(1)}, bf16[16,2176]{1,0:T(8,128)(2,1)S(1)}, u32[]{:S(2)}, u32[]{:S(2)}) %collective-permute-start.1) | collective-permute-done | bytes 69664 | tf_op jit(solution)/shard_map/ppermute | solution.py:282
  20.6 0.0 collective-permute-done
  20.7 1.6 %collective-permute-start.3 = (bf16[4,16,2176]{2,1,0:T(8,128)(2,1)S(1)}, bf16[4,16,2176]{2,1,0:T(8,128)(2,1)S(1)}, u32[]{:S(2)}, u32[]{:S(2)}) collective-permute-start(bf16[4,16,2176]{2,1,0:T(8,128)(2,1)S(1)} %pad_maximum_fusion.refs_2_), channel_id=1, source_target_pairs={{0,2},{1,3},{2,0},{3,1},{4,6},{5,7},{6,4},{7,5},{8,10},{9,11},{10,... | collective-permute-start | bytes 835592 | tf_op jit(solution)/shard_map/ppermute | solution.py:282
  22.3 0.0 collective-permute-start.4
  22.3 6.5 %collective-permute-done.3.refs_3_ = bf16[4,16,2176]{2,1,0:T(8,128)(2,1)S(1)} collective-permute-done((bf16[4,16,2176]{2,1,0:T(8,128)(2,1)S(1)}, bf16[4,16,2176]{2,1,0:T(8,128)(2,1)S(1)}, u32[]{:S(2)}, u32[]{:S(2)}) %collective-permute-start.3) | collective-permute-done | bytes 278560 | tf_op jit(solution)/shard_map/ppermute | solution.py:282
  28.8 0.0 collective-permute-start.5
  28.8 0.0 collective-permute-done.4.refs_4_
  28.8 1.6 %collective-permute-done.5.refs_5_ = bf16[4,16,2176]{2,1,0:T(8,128)(2,1)S(1)} collective-permute-done((bf16[4,16,2176]{2,1,0:T(8,128)(2,1)S(1)}, bf16[4,16,2176]{2,1,0:T(8,128)(2,1)S(1)}, u32[]{:S(2)}, u32[]{:S(2)}) %collective-permute-start.5) | collective-permute-done | bytes 278560 | tf_op jit(solution)/shard_map/ppermute | solution.py:282
  30.4 5.8 %feed_forward.1 = (bf16[2,16,2048]{2,1,0:T(8,128)(2,1)S(1)}, bf16[2,16,2048]{2,1,0:T(8,128)(2,1)S(1)}, bf16[2,16,2048]{2,1,0:T(8,128)(2,1)S(1)}, bf16[2,16,2048]...) custom-call(s32[1]{0:T(128)} %bitcast.5.refs_0_, f32[1,2048]{1,0:T(1,128)} %bitcast.42, ...), custom_call_target="tpu_custom_call" | custom-call | tf_op jit(solution)/shard_map/feed_forward/pallas_call | solution.py:262
  36.1 0.2 collective-permute-start.6
  36.3 1.8 %collective-permute-done.6 = bf16[8,16,2048]{2,1,0:T(8,128)(2,1)S(1)} collective-permute-done((bf16[8,16,2048]{2,1,0:T(8,128)(2,1)S(1)}, bf16[8,16,2048]{2,1,0:T(8,128)(2,1)S(1)}, u32[]{:S(2)}, u32[]{:S(2)}) %collective-permute-start.6) | collective-permute-done | bytes 524320 | tf_op jit(solution)/shard_map/ppermute | solution.py:282
  38.2 1.8 %collective-permute-start.8 = (bf16[2,16,2048]{2,1,0:T(8,128)(2,1)S(1)}, bf16[2,16,2048]{2,1,0:T(8,128)(2,1)S(1)}, u32[]{:S(2)}, u32[]{:S(2)}) collective-permute-start(bf16[2,16,2048]{2,1,0:T(8,128)(2,1)S(1)} %add_convert_fusion.1), channel_id=1, source_target_pairs={{0,2},{1,3},{2,0},{3,1},{4,6},{5,7},{6,4},{7,5},{8,10},{9,11},{10,... | collective-permute-start | bytes 393224 | tf_op jit(solution)/shard_map/ppermute | solution.py:282
  39.9 3.8 %collective-permute-done.8 = bf16[2,16,2048]{2,1,0:T(8,128)(2,1)S(1)} collective-permute-done((bf16[2,16,2048]{2,1,0:T(8,128)(2,1)S(1)}, bf16[2,16,2048]{2,1,0:T(8,128)(2,1)S(1)}, u32[]{:S(2)}, u32[]{:S(2)}) %collective-permute-start.8) | collective-permute-done | bytes 131104 | tf_op jit(solution)/shard_map/ppermute | solution.py:282
  43.8 0.1 add_convert_fusion
  43.8 1.8 %collective-permute-start.7 = (bf16[2,16,2048]{2,1,0:T(8,128)(2,1)S(1)}, bf16[2,16,2048]{2,1,0:T(8,128)(2,1)S(1)}, u32[]{:S(2)}, u32[]{:S(2)}) collective-permute-start(bf16[2,16,2048]{2,1,0:T(8,128)(2,1)S(1)} %get-tuple-element.20), channel_id=1, source_target_pairs={{0,2},{1,3},{2,0},{3,1},{4,6},{5,7},{6,4},{7,5},{8,10},{9,11},{10,... | collective-permute-start | bytes 393224 | tf_op jit(solution)/shard_map/ppermute | solution.py:282
  45.6 0.1 collective-permute-start.9
  45.8 2.4 %collective-permute-start.10 = (bf16[16,2048]{1,0:T(8,128)(2,1)S(1)}, bf16[16,2048]{1,0:T(8,128)(2,1)S(1)}, u32[]{:S(2)}, u32[]{:S(2)}) collective-permute-start(bf16[16,2048]{1,0:T(8,128)(2,1)S(1)} %get-tuple-element.22), channel_id=1, source_target_pairs={{0,12},{1,13},{2,14},{3,15},{4,8},{5,9},{6,10},{7,11},{8,4},{9,5},... | collective-permute-start | bytes 196616 | tf_op jit(solution)/shard_map/ppermute | solution.py:282
  48.2 0.7 %collective-permute-done.7 = bf16[2,16,2048]{2,1,0:T(8,128)(2,1)S(1)} collective-permute-done((bf16[2,16,2048]{2,1,0:T(8,128)(2,1)S(1)}, bf16[2,16,2048]{2,1,0:T(8,128)(2,1)S(1)}, u32[]{:S(2)}, u32[]{:S(2)}) %collective-permute-start.7) | collective-permute-done | bytes 131104 | tf_op jit(solution)/shard_map/ppermute | solution.py:282
  48.9 0.4 collective-permute-start.11
  49.3 3.3 %collective-permute-done.9 = bf16[16,2048]{1,0:T(8,128)(2,1)S(1)} collective-permute-done((bf16[16,2048]{1,0:T(8,128)(2,1)S(1)}, bf16[16,2048]{1,0:T(8,128)(2,1)S(1)}, u32[]{:S(2)}, u32[]{:S(2)}) %collective-permute-start.9) | collective-permute-done | bytes 65568 | tf_op jit(solution)/shard_map/ppermute | solution.py:282
  52.6 0.0 collective-permute-done.10
  52.6 0.7 %collective-permute-done.11 = bf16[16,2048]{1,0:T(8,128)(2,1)S(1)} collective-permute-done((bf16[16,2048]{1,0:T(8,128)(2,1)S(1)}, bf16[16,2048]{1,0:T(8,128)(2,1)S(1)}, u32[]{:S(2)}, u32[]{:S(2)}) %collective-permute-start.11) | collective-permute-done | bytes 65568 | tf_op jit(solution)/shard_map/ppermute | solution.py:282
  53.3 0.7 %fusion.4 = bf16[16,2048]{1,0:T(8,128)(2,1)} fusion(f32[16,2048]{1,0:T(8,128)S(1)} %get-tuple-element.12, f32[2,16,2048]{2,1,0:T(8,128)S(1)} %convert_add_fusion, bf16[16,2048]{1,0:T(8,128)(2,1)S(1)} %collective-permute-done.11, bf16[16,2048]{1,0:T(8,128)(2,1)S(1)} %collective-permute-done.10, bf16[16,2048]{1,0:T(8,128)(2,1)S(1)} %collective-permute-done.9), kind=kLoop, calls=%fused_computation.11 | loop fusion | flops 262144 | bytes 524288 | tf_op jit(solution)/shard_map/convert_element_type | solution.py:336
  (5 shorter events, 0.1 us)
Async XLA Ops:
  9.6 7.7 %collective-permute-start.2 = (bf16[16,2176]{1,0:T(8,128)(2,1)S(1)}, bf16[16,2176]{1,0:T(8,128)(2,1)S(1)}, u32[]{:S(2)}, u32[]{:S(2)}) collective-permute-start(bf16[16,2176]{1,0:T(8,128)(2,1)S(1)} %get-tuple-element.13), channel_id=1, source_target_pairs={{0,12},{1,13},{2,14},{3,15},{4,8},{5,9},{6,10},{7,11},{8,4},{9,5},... | collective-permute-start | bytes 208904 | tf_op jit(solution)/shard_map/ppermute | solution.py:282
  14.7 5.9 %collective-permute-start.1 = (bf16[16,2176]{1,0:T(8,128)(2,1)S(1)}, bf16[16,2176]{1,0:T(8,128)(2,1)S(1)}, u32[]{:S(2)}, u32[]{:S(2)}) collective-permute-start(bf16[16,2176]{1,0:T(8,128)(2,1)S(1)} %get-tuple-element.13), channel_id=1, source_target_pairs={{0,8},{1,9},{2,10},{3,11},{4,12},{5,13},{6,14},{7,15},{8,0},{9,1},... | collective-permute-start | bytes 208904 | tf_op jit(solution)/shard_map/ppermute | solution.py:282
  14.7 5.9 %collective-permute-start = (bf16[16,2176]{1,0:T(8,128)(2,1)S(1)}, bf16[16,2176]{1,0:T(8,128)(2,1)S(1)}, u32[]{:S(2)}, u32[]{:S(2)}) collective-permute-start(bf16[16,2176]{1,0:T(8,128)(2,1)S(1)} %get-tuple-element.13), channel_id=1, source_target_pairs={{0,4},{1,5},{2,6},{3,7},{4,0},{5,1},{6,2},{7,3},{8,12},{9,13},{10,... | collective-permute-start | bytes 208904 | tf_op jit(solution)/shard_map/ppermute | solution.py:282
  20.7 8.1 %collective-permute-start.3 = (bf16[4,16,2176]{2,1,0:T(8,128)(2,1)S(1)}, bf16[4,16,2176]{2,1,0:T(8,128)(2,1)S(1)}, u32[]{:S(2)}, u32[]{:S(2)}) collective-permute-start(bf16[4,16,2176]{2,1,0:T(8,128)(2,1)S(1)} %pad_maximum_fusion.refs_2_), channel_id=1, source_target_pairs={{0,2},{1,3},{2,0},{3,1},{4,6},{5,7},{6,4},{7,5},{8,10},{9,11},{10,... | collective-permute-start | bytes 835592 | tf_op jit(solution)/shard_map/ppermute | solution.py:282
  22.3 6.5 %collective-permute-start.4 = (bf16[4,16,2176]{2,1,0:T(8,128)(2,1)S(1)}, bf16[4,16,2176]{2,1,0:T(8,128)(2,1)S(1)}, u32[]{:S(2)}, u32[]{:S(2)}) collective-permute-start(bf16[4,16,2176]{2,1,0:T(8,128)(2,1)S(1)} %pad_maximum_fusion.refs_2_), channel_id=1, source_target_pairs={{0,1},{1,0},{2,3},{3,2},{4,5},{5,4},{6,7},{7,6},{8,9},{9,8},{10,11... | collective-permute-start | bytes 835592 | tf_op jit(solution)/shard_map/ppermute | solution.py:282
  28.8 1.6 %collective-permute-start.5 = (bf16[4,16,2176]{2,1,0:T(8,128)(2,1)S(1)}, bf16[4,16,2176]{2,1,0:T(8,128)(2,1)S(1)}, u32[]{:S(2)}, u32[]{:S(2)}) collective-permute-start(bf16[4,16,2176]{2,1,0:T(8,128)(2,1)S(1)} %collective-permute-done.3.refs_3_), channel_id=1, source_target_pairs={{0,1},{1,0},{2,3},{3,2},{4,5},{5,4},{6,7},{7,6},{8,9},{9,8},{10,11... | collective-permute-start | bytes 835592 | tf_op jit(solution)/shard_map/ppermute | solution.py:282
  36.1 2.0 %collective-permute-start.6 = (bf16[8,16,2048]{2,1,0:T(8,128)(2,1)S(1)}, bf16[8,16,2048]{2,1,0:T(8,128)(2,1)S(1)}, u32[]{:S(2)}, u32[]{:S(2)}) collective-permute-start(bf16[8,16,2048]{2,1,0:T(8,128)(2,1)S(1)} %get-tuple-element.15), channel_id=1, source_target_pairs={{0,1},{1,0},{2,3},{3,2},{4,5},{5,4},{6,7},{7,6},{8,9},{9,8},{10,11... | collective-permute-start | bytes 1572872 | tf_op jit(solution)/shard_map/ppermute | solution.py:282
  38.2 5.6 %collective-permute-start.8 = (bf16[2,16,2048]{2,1,0:T(8,128)(2,1)S(1)}, bf16[2,16,2048]{2,1,0:T(8,128)(2,1)S(1)}, u32[]{:S(2)}, u32[]{:S(2)}) collective-permute-start(bf16[2,16,2048]{2,1,0:T(8,128)(2,1)S(1)} %add_convert_fusion.1), channel_id=1, source_target_pairs={{0,2},{1,3},{2,0},{3,1},{4,6},{5,7},{6,4},{7,5},{8,10},{9,11},{10,... | collective-permute-start | bytes 393224 | tf_op jit(solution)/shard_map/ppermute | solution.py:282
  43.8 5.0 %collective-permute-start.7 = (bf16[2,16,2048]{2,1,0:T(8,128)(2,1)S(1)}, bf16[2,16,2048]{2,1,0:T(8,128)(2,1)S(1)}, u32[]{:S(2)}, u32[]{:S(2)}) collective-permute-start(bf16[2,16,2048]{2,1,0:T(8,128)(2,1)S(1)} %get-tuple-element.20), channel_id=1, source_target_pairs={{0,2},{1,3},{2,0},{3,1},{4,6},{5,7},{6,4},{7,5},{8,10},{9,11},{10,... | collective-permute-start | bytes 393224 | tf_op jit(solution)/shard_map/ppermute | solution.py:282
  45.6 7.0 %collective-permute-start.9 = (bf16[16,2048]{1,0:T(8,128)(2,1)S(1)}, bf16[16,2048]{1,0:T(8,128)(2,1)S(1)}, u32[]{:S(2)}, u32[]{:S(2)}) collective-permute-start(bf16[16,2048]{1,0:T(8,128)(2,1)S(1)} %get-tuple-element.21), channel_id=1, source_target_pairs={{0,8},{1,9},{2,10},{3,11},{4,12},{5,13},{6,14},{7,15},{8,0},{9,1},... | collective-permute-start | bytes 196616 | tf_op jit(solution)/shard_map/ppermute | solution.py:282
  45.8 6.9 %collective-permute-start.10 = (bf16[16,2048]{1,0:T(8,128)(2,1)S(1)}, bf16[16,2048]{1,0:T(8,128)(2,1)S(1)}, u32[]{:S(2)}, u32[]{:S(2)}) collective-permute-start(bf16[16,2048]{1,0:T(8,128)(2,1)S(1)} %get-tuple-element.22), channel_id=1, source_target_pairs={{0,12},{1,13},{2,14},{3,15},{4,8},{5,9},{6,10},{7,11},{8,4},{9,5},... | collective-permute-start | bytes 196616 | tf_op jit(solution)/shard_map/ppermute | solution.py:282
  48.9 4.4 %collective-permute-start.11 = (bf16[16,2048]{1,0:T(8,128)(2,1)S(1)}, bf16[16,2048]{1,0:T(8,128)(2,1)S(1)}, u32[]{:S(2)}, u32[]{:S(2)}) collective-permute-start(bf16[16,2048]{1,0:T(8,128)(2,1)S(1)} %fusion.5), channel_id=1, source_target_pairs={{0,4},{1,5},{2,6},{3,7},{4,0},{5,1},{6,2},{7,3},{8,12},{9,13},{10,... | collective-permute-start | bytes 196616 | tf_op jit(solution)/shard_map/ppermute | solution.py:282
